TPU v7x, 32 devices: a whole 2x2x4 slice. The times are simulated.
32 devices in a mesh: grp: 2 (over y), ep: 4 (over z), tp: 4 (over x, core).
Axes of the slice: x: 2, y: 2, z: 4, core: 2. Of those that a mesh axis runs over, the one named last changes fastest.
Arguments:
- out_gate: bfloat16 [1536, 4096], P(('grp', 'ep'), 'tp'), parts along dimension 0, may hold values from -6 to 6
- in_gate: bfloat16 [1536, 4096], P(('grp', 'ep'), 'tp'), parts along dimension 0, may hold values from -6 to 6
- values: bfloat16 [1536, 4096], P(('grp', 'ep'), 'tp'), parts along dimension 0, may hold values from -6 to 6
- conv_taps: float32 [3, 4096], P(None, 'tp'), may hold values from -3 to 3
- mixer_weight: bfloat16 [4096, 4096], P(None, 'tp'), may hold values from -0.09375 to 0.09375
- expert_input: bfloat16 [1536, 4096], P(('grp', 'ep', 'tp')), parts along dimension 0, may hold values from -6 to 6
- norm_gain: float32 [4096], replicated, may hold values from 0.1 to 1.9
- route_ids: int32 [1536, 2], P(('grp', 'ep')), parts along dimension 0, may hold values from 0 to 3, all different within a row; in each aligned block of 48 rows (0 to 47, 48 to 95, ...) at most 48 rows name the same one
- route_weights: float32 [1536, 2], P(('grp', 'ep')), parts along dimension 0, may hold values from 0.25 to 1.25
- gate_weight: bfloat16 [4, 4096, 1024], P('ep', None, 'tp'), may hold values from -0.09375 to 0.09375
- up_weight: bfloat16 [4, 4096, 1024], P('ep', None, 'tp'), may hold values from -0.09375 to 0.09375
- down_weight: bfloat16 [4, 1024, 4096], P('ep', None, 'tp'), may hold values from -0.1875 to 0.1875
- shared_gate: bfloat16 [4096, 512], P(None, 'tp'), may hold values from -0.09375 to 0.09375
- shared_up: bfloat16 [4096, 512], P(None, 'tp'), may hold values from -0.09375 to 0.09375
- shared_down: bfloat16 [512, 4096], P(None, 'tp'), may hold values from -0.25 to 0.25
Outputs:
- mixer_output: bfloat16 [1536, 4096], P(('grp', 'ep'), 'tp'), parts along dimension 0
- expert_output: bfloat16 [1536, 4096], P(('grp', 'ep'), 'tp'), parts along dimension 0
There are 2 independent parts, one for each index of `grp`. A program takes and returns all parts, laid end to end along the dimension named above; an argument that names none is the same for every part. Nothing has to cross between parts.
Inputs may be any that keep to these rules, and one draw needn't show every extreme that they name: `route_ids`: the 2 entries of a row differ. In each aligned block of 48 rows (the routed tokens of one device) no expert is named by more than 48 rows, and in some block an expert is named by exactly 48 rows.
All inputs are finite; a program needn't handle non-finite values.
Results may differ from a plain program's by a relative error of at most 0.0067.
Values may be sent and summed in bfloat16 or wider, within the bound.
A program may use at most 64 MiB of HBM per device.

v0:
```python
import functools

import jax
import jax.numpy as jnp
from jax import lax
from jax.experimental import pallas as pl
from jax.experimental.pallas import tpu as pltpu
from jax.sharding import PartitionSpec as P

MESH = pl.DeviceIdType.MESH
CORES = 2
TILE = 256
PIECE = 16
CHUNKS = 4

norm_floor = 0.5


def shifted(value, axis, steps):
    count = lax.axis_size(axis)
    leading, last = (max(0, -steps), min(count, count - steps))
    return lax.ppermute(value, axis, [(source, source + steps) for source in range(leading, last)])


def layer_norm(tokens, norm_gain):
    widened = tokens.astype(jnp.float32)
    centred = widened - jnp.mean(widened, axis=-1, keepdims=True)
    spread = jnp.mean(centred * centred, axis=-1, keepdims=True)
    return (centred * lax.rsqrt(spread + norm_floor) * norm_gain).astype(jnp.bfloat16)


def expert_hidden(inputs, gate_part, up_part):
    gate_value = jnp.dot(inputs, gate_part, preferred_element_type=jnp.float32)
    up_value = jnp.dot(inputs, up_part, preferred_element_type=jnp.float32)
    return (jax.nn.silu(gate_value) * up_value).astype(jnp.bfloat16)


def slot_ranks(route_ids, experts, lanes):
    tok_count, top_count = route_ids.shape
    grouped = route_ids.reshape(lanes, tok_count // lanes * top_count)
    onehot = (grouped[:, :, None] == jnp.arange(experts, dtype=jnp.int32)[None, None, :]).astype(
        jnp.int32
    )
    before = jnp.cumsum(onehot, axis=1) - onehot
    return jnp.sum(before * onehot, axis=2).reshape(tok_count, top_count)


def plain(
    out_gate,
    in_gate,
    values,
    conv_taps,
    mixer_weight,
    expert_input,
    norm_gain,
    route_ids,
    route_weights,
    gate_weight,
    up_weight,
    down_weight,
    shared_gate,
    shared_up,
    shared_down,
):
    experts = lax.axis_size("ep")
    lanes = lax.axis_size("tp")
    lane_rows = expert_input.shape[0]
    width = expert_input.shape[1]
    tok_count, top_count = route_ids.shape
    capacity = (2 * lane_rows * top_count + experts - 1) // experts
    gated_values = (in_gate.astype(jnp.float32) * values.astype(jnp.float32)).astype(jnp.bfloat16)
    previous = shifted(gated_values[-2:], "ep", 1)
    extended = jnp.concatenate([previous, gated_values], axis=0).astype(jnp.float32)
    conv_state = (
        conv_taps[0] * extended[:-2] + conv_taps[1] * extended[1:-1] + conv_taps[2] * extended[2:]
    )
    mixed_rows = (out_gate.astype(jnp.float32) * conv_state).astype(jnp.bfloat16)
    normed_own = layer_norm(expert_input, norm_gain)
    mixed_whole, normed_rows = (
        lax.all_gather(mixed_rows, "tp", axis=1, tiled=True),
        lax.all_gather(normed_own, "tp", axis=0, tiled=True),
    )
    mixer_output = jnp.dot(mixed_whole, mixer_weight, preferred_element_type=jnp.float32).astype(
        jnp.bfloat16
    )
    shared_part = expert_hidden(normed_rows, shared_gate, shared_up)
    slot_index = slot_ranks(route_ids, experts, lanes)
    lane_of_row = (jnp.arange(tok_count, dtype=jnp.int32) // lane_rows)[:, None]
    positions = (route_ids * lanes + lane_of_row) * capacity + slot_index
    lane_index = lax.axis_index("tp")
    lane_ids = lax.dynamic_slice_in_dim(route_ids, lane_index * lane_rows, lane_rows, 0)
    lane_slots = lax.dynamic_slice_in_dim(slot_index, lane_index * lane_rows, lane_rows, 0)
    lane_places = lane_ids * capacity + lane_slots
    local_rows = jnp.broadcast_to(jnp.arange(lane_rows, dtype=jnp.int32)[:, None], lane_ids.shape)
    owners = jnp.full((experts * capacity,), lane_rows, jnp.int32)
    owners = owners.at[lane_places.reshape(-1)].set(local_rows.reshape(-1))
    outgoing = jnp.take(normed_own, owners, axis=0, mode="fill", fill_value=0)
    arrived = lax.all_to_all(
        outgoing.reshape(experts, capacity, width), "ep", split_axis=0, concat_axis=0, tiled=True
    )
    segment = lax.all_gather(arrived[None], "tp", axis=0, tiled=True)
    hidden_rows = expert_hidden(segment.reshape(-1, width), gate_weight[0], up_weight[0])
    spread_hidden = hidden_rows.reshape(segment.shape[:-1] + (hidden_rows.shape[-1],))
    routed_hidden = jnp.swapaxes(spread_hidden, 0, 1).reshape(-1, spread_hidden.shape[-1])
    routed_whole, shared_whole = (
        lax.all_gather(routed_hidden, "tp", axis=1, tiled=True),
        lax.all_gather(shared_part, "tp", axis=1, tiled=True),
    )
    routed_result = jnp.dot(
        routed_whole, down_weight[0], preferred_element_type=jnp.float32
    ).astype(jnp.bfloat16)
    out_cols = routed_result.shape[-1]
    returned = lax.all_to_all(
        routed_result.reshape(experts, lanes * capacity, out_cols),
        "ep",
        split_axis=0,
        concat_axis=0,
        tiled=True,
    )
    shared_result = jnp.dot(shared_whole, shared_down, preferred_element_type=jnp.float32)
    picked = jnp.take(
        returned.reshape(experts * lanes * capacity, out_cols), positions.reshape(-1), axis=0
    )
    picked = picked.astype(jnp.float32).reshape(tok_count, top_count, out_cols)
    expert_output = (shared_result + jnp.sum(route_weights[:, :, None] * picked, axis=1)).astype(
        jnp.bfloat16
    )
    return (mixer_output, expert_output)


def silu_product(gate_value, up_value):
    return (gate_value * (1.0 / (1.0 + jnp.exp(-gate_value))) * up_value).astype(jnp.bfloat16)


def dot32(left, right):
    return jnp.dot(left, right, preferred_element_type=jnp.float32)


def kernel(
    n_ep,
    n_tp,
    ids,
    rw,
    og_h,
    ig_h,
    va_h,
    taps_h,
    mw_h,
    ei_h,
    ng_h,
    gw_h,
    uw_h,
    dw_h,
    sg_h,
    su_h,
    sd_h,
    mix_out,
    exp_out,
    og,
    ig,
    va,
    taps,
    mw,
    ei,
    ng,
    gw,
    uw,
    dw,
    sg,
    su,
    sd,
    tok,
    hid,
    shd,
    mixed,
    gated,
    halo,
    res,
    pin,
    wts,
    ld,
    z_send,
    z_recv,
    x_send,
    x_recv,
    p_send,
    p_recv,
    r_send,
    r_recv,
    w_send,
    w_recv,
    h_sem,
):
    e = lax.axis_index("ep")
    t = lax.axis_index("tp")
    n_x = n_tp // CORES
    partner = t + 1 - 2 * (t % CORES)
    lane_rows, width = ei.shape
    rows, chans = og.shape

    loads = {}
    for number, (name, src, dst) in enumerate(
        (
            ("ei", ei_h, ei),
            ("ng", ng_h, ng),
            ("ig", ig_h, ig),
            ("va", va_h, va),
            ("og", og_h, og),
            ("taps", taps_h, taps),
            ("gw", gw_h, gw),
            ("uw", uw_h, uw),
            ("sg", sg_h, sg),
            ("su", su_h, su),
            ("dw", dw_h, dw),
            ("sd", sd_h, sd),
            ("mw", mw_h, mw),
        )
    ):
        loads[name] = pltpu.make_async_copy(src, dst, ld.at[number])
        loads[name].start()

    barrier = pltpu.get_barrier_semaphore()
    greeted = [{"ep": (e + d) % n_ep, "tp": t} for d in range(1, n_ep)]
    greeted += [{"ep": e, "tp": (t + CORES * d) % n_tp} for d in range(1, n_x)]
    greeted += [{"ep": e, "tp": partner}]
    for peer in greeted:
        pl.semaphore_signal(barrier, inc=1, device_id=peer, device_id_type=MESH)

    def remote(src, dst, send, recv, ep, tp):
        return pltpu.make_async_remote_copy(
            src_ref=src,
            dst_ref=dst,
            send_sem=send,
            recv_sem=recv,
            device_id={"ep": ep, "tp": tp},
            device_id_type=MESH,
        )

    def cross(slot, g, d, lane):
        return remote(
            slot(lane), slot(lane), x_send.at[g, d - 1], x_recv.at[g, d - 1],
            e, (t + CORES * d) % n_tp,
        )

    def across(slot, g, d, lane):
        return remote(slot(lane), slot(lane), p_send.at[g, d], p_recv.at[g, d], e, partner)

    def from_x(d):
        return (t + n_tp - CORES * d) % n_tp

    def from_partner(d):
        return (partner + n_tp - CORES * d) % n_tp

    def gather_start(slot, g):
        for d in range(1, n_x):
            cross(slot, g, d, t).start()
        across(slot, g, 0, t).start()

    def gather_forward(slot, g):
        for d in range(1, n_x):
            cross(slot, g, d, from_x(d)).wait_recv()
            across(slot, g, d, from_x(d)).start()

    def gather_finish(slot, g):
        for d in range(n_x):
            across(slot, g, d, from_partner(d)).wait_recv()

    def gather_drain(slot, g):
        for d in range(1, n_x):
            cross(slot, g, d, t).wait_send()
            across(slot, g, d, from_x(d)).wait_send()
        across(slot, g, 0, t).wait_send()

    pieces = lane_rows // PIECE
    first_hidden = n_ep * pieces
    shared_g = first_hidden + n_ep
    mixed_g = shared_g + 1

    def tok_slot(j, q):
        return lambda lane: tok.at[j, lane, q]

    def hid_slot(j):
        return lambda lane: hid.at[j, lane]

    def shd_slot(lane):
        return shd.at[lane]

    def mixed_slot(lane):
        return mixed.at[lane]

    nearest = jnp.minimum(e, n_ep - 1 - e)
    left_short = e <= n_ep - 1 - e

    def block_at(k):
        near = jnp.where(k % 2 == 1, e - (k + 1) // 2, e + k // 2)
        far = jnp.where(left_short, k, n_ep - 1 - k)
        return jnp.where(k <= 2 * nearest, near, far)

    def at_end(j):
        return (j == 0) | (j == n_ep - 1)

    def crosses(j):
        return (j == e) | ~at_end(j)

    def z_copy(side, d, j, q):
        block = tok.at[j, from_x(d), q]
        return remote(block, block, z_send.at[side, d, j, q], z_recv.at[d, j, q],
                      jnp.clip(e + 1 - 2 * side, 0, n_ep - 1), t)

    def goes_right(j):
        return (j <= e) & (e < n_ep - 1)

    def goes_left(j):
        return (j >= e) & (e > 0)

    def z_onward(d, j, q):
        @pl.when(goes_right(j))
        def _():
            z_copy(0, d, j, q).start()

        @pl.when(goes_left(j))
        def _():
            z_copy(1, d, j, q).start()

    def spread(k, q):
        j = block_at(k)
        g = j * pieces + q

        @pl.when(k > 0)
        def _():
            z_copy(0, 0, j, q).wait_recv()

        z_onward(0, j, q)

        @pl.when(crosses(j))
        def _():
            for d in range(1, n_x):
                cross(tok_slot(j, q), g, d, t).start()

        across(tok_slot(j, q), g, 0, t).start()

    def forward(k, q):
        j = block_at(k)
        g = j * pieces + q
        for d in range(1, n_x):

            @pl.when(crosses(j))
            def _():
                cross(tok_slot(j, q), g, d, from_x(d)).wait_recv()

            @pl.when(~crosses(j))
            def _():
                z_copy(0, d, j, q).wait_recv()

            @pl.when(at_end(j))
            def _():
                z_onward(d, j, q)

            across(tok_slot(j, q), g, d, from_x(d)).start()

    piece = rows // CHUNKS

    def hop(j, c):
        at = pl.ds(pl.multiple_of(c * piece, 16), piece)
        after = jnp.clip(jnp.where(j > e, e + 1, e - 1), 0, n_ep - 1)
        slot = jnp.where((j < e) & (after == j), n_ep, j)
        return remote(res.at[j, at], pin.at[slot, at], r_send.at[j, c], r_recv.at[slot, c], after, t)

    def hop_arrives(slot, c):
        at = pl.ds(pl.multiple_of(c * piece, 16), piece)
        remote(res.at[0, at], pin.at[slot, at], r_send.at[0, c], r_recv.at[slot, c],
               jnp.clip(e + 1, 0, n_ep - 1), t).wait_recv()

    inner = (e > 0) & (e < n_ep - 1)

    def weights_to(d):
        return remote(wts.at[e], wts.at[e], w_send.at[d - 1], w_recv.at[e], (e + d) % n_ep, t)

    def weight_column(j):
        held = wts[j]
        mine = jnp.where(lax.broadcasted_iota(jnp.int32, held.shape, 0) == e, held, 0.0)
        line = jnp.sum(mine, axis=0, keepdims=True)
        shape = (rows, held.shape[1])
        same = lax.broadcasted_iota(jnp.int32, shape, 0) == lax.broadcasted_iota(jnp.int32, shape, 1)
        return jnp.sum(jnp.where(same, line, 0.0), axis=1, keepdims=True)

    loads["ei"].wait()
    loads["ng"].wait()

    def norm_rows(r, _):
        at = pl.ds(pl.multiple_of(r * PIECE, PIECE), PIECE)
        widened = ei[at, :].astype(jnp.float32)
        centred = widened - jnp.mean(widened, axis=-1, keepdims=True)
        spread_of = jnp.mean(centred * centred, axis=-1, keepdims=True)
        normed = centred * lax.rsqrt(spread_of + norm_floor) * ng[...]
        tok[e, t, r] = normed.astype(jnp.bfloat16)
        return 0

    lax.fori_loop(0, pieces, norm_rows, 0)
    pl.semaphore_wait(barrier, len(greeted))
    for q in range(pieces):
        spread(0, q)

    place = lax.broadcasted_iota(jnp.int32, (wts.shape[1], rows), 0)
    dense = jnp.zeros(place.shape, jnp.float32)
    for k in range(ids.shape[0]):
        dense += jnp.where(ids[k : k + 1, :] == place, rw[k : k + 1, :], 0.0)
    wts[e] = jnp.zeros(wts.shape[1:], jnp.float32)
    wts[e, :, 0:rows] = dense
    for d in range(1, n_ep):
        weights_to(d).start()

    loads["ig"].wait()
    loads["va"].wait()

    def gate_cols(c, _):
        at = pl.ds(pl.multiple_of(c * 128, 128), 128)
        gated[:, at] = (ig[:, at].astype(jnp.float32) * va[:, at].astype(jnp.float32)).astype(
            jnp.bfloat16
        )
        return 0

    lax.fori_loop(0, chans // 128, gate_cols, 0)

    def halo_copy():
        return remote(gated.at[pl.ds(rows - 16, 16)], halo, h_sem.at[0], h_sem.at[1],
                      jnp.minimum(e + 1, n_ep - 1), t)

    @pl.when(e < n_ep - 1)
    def _():
        halo_copy().start()

    loads["og"].wait()
    loads["taps"].wait()

    @pl.when(e == 0)
    def _():
        halo[...] = jnp.zeros_like(halo)

    @pl.when(e > 0)
    def _():
        halo_copy().wait_recv()

    def mix_cols(c, _):
        at = pl.ds(pl.multiple_of(c * 128, 128), 128)
        now = gated[:, at].astype(jnp.float32)
        before = halo[:, at].astype(jnp.float32)
        place = lax.broadcasted_iota(jnp.int32, now.shape, 0)
        one = jnp.where(place == 0, before[15:16], pltpu.roll(now, 1, 0))
        two = jnp.where(
            place == 0, before[14:15], jnp.where(place == 1, before[15:16], pltpu.roll(now, 2, 0))
        )
        state = taps[0:1, at] * two + taps[1:2, at] * one + taps[2:3, at] * now
        mixed[t, :, at] = (og[:, at].astype(jnp.float32) * state).astype(jnp.bfloat16)
        return 0

    lax.fori_loop(0, chans // 128, mix_cols, 0)
    for name in ("gw", "uw", "sg", "su"):
        loads[name].wait()

    def leave(k, _):
        j = block_at(k)
        gather_forward(hid_slot(j), first_hidden + j)
        gather_finish(hid_slot(j), first_hidden + j)
        part = hid.shape[-1]

        @pl.when(j != e)
        def _():
            remote(wts.at[e], wts.at[j], w_send.at[0], w_recv.at[j], j, t).wait_recv()

        weight = weight_column(j)
        for c in range(chans // TILE):
            at = slice(c * TILE, (c + 1) * TILE)
            total = dot32(hid[j, 0], dw[0:part, at])
            for lane in range(1, n_tp):
                total += dot32(hid[j, lane], dw[lane * part : (lane + 1) * part, at])
            res[j, :, at] = (weight * total).astype(jnp.bfloat16)

        @pl.when((j != e) & ~inner)
        def _():
            for c in range(CHUNKS):
                hop(j, c).start()
        return 0

    def meet(k):
        j = block_at(k)
        for q in range(pieces):
            gather_finish(tok_slot(j, q), j * pieces + q)
        block = tok[j].reshape(rows, width)
        hid[j, t] = silu_product(dot32(block, gw[...]), dot32(block, uw[...]))
        gather_start(hid_slot(j), first_hidden + j)

        @pl.when(k == 0)
        def _():
            block = tok[e].reshape(rows, width)
            shd[t] = silu_product(dot32(block, sg[...]), dot32(block, su[...]))
            gather_start(shd_slot, shared_g)
            loads["dw"].wait()

        @pl.when(k == n_ep - 1)
        def _():
            gather_start(mixed_slot, mixed_g)

    def step(s, _):
        for q in range(pieces):

            @pl.when(s + 1 < n_ep)
            def _():
                spread(s + 1, q)

            @pl.when(s < n_ep)
            def _():
                forward(s, q)

        @pl.when(~inner)
        def _():
            lax.fori_loop(jnp.maximum(s - 1, 0), s, leave, 0)

        k = jnp.where(inner, s - 1, s)

        @pl.when((k >= 0) & (k < n_ep))
        def _():
            meet(k)

        @pl.when(inner & (s == n_ep))
        def _():
            lax.fori_loop(0, n_ep, leave, 0)

        return 0

    lax.fori_loop(0, n_ep + 1, step, 0)

    gather_forward(shd_slot, shared_g)

    for phase in range(2):
        right = left_short if phase == 0 else ~left_short

        def relay(d, _):
            j = jnp.where(right, e + d, e - d)

            @pl.when(inner & (j >= 0) & (j < n_ep))
            def _():
                def relay_piece(c, _):
                    at = pl.ds(pl.multiple_of(c * piece, 16), piece)
                    hop_arrives(j, c)
                    total = res[j, at, :].astype(jnp.float32) + pin[j, at, :].astype(jnp.float32)
                    res[j, at, :] = total.astype(jnp.bfloat16)
                    hop(j, c).start()
                    return 0

                lax.fori_loop(0, CHUNKS, relay_piece, 0)

            return 0

        lax.fori_loop(1, n_ep, relay, 0)

    gather_forward(mixed_slot, mixed_g)
    gather_finish(shd_slot, shared_g)
    loads["sd"].wait()
    loads["mw"].wait()
    gather_finish(mixed_slot, mixed_g)

    def mixer_cols(c, _):
        at = pl.ds(pl.multiple_of(c * TILE, TILE), TILE)
        total = dot32(mixed[0], mw[0:chans, at])
        for lane in range(1, n_tp):
            total += dot32(mixed[lane], mw[lane * chans : (lane + 1) * chans, at])
        mix_out[:, at] = total.astype(jnp.bfloat16)
        return 0

    lax.fori_loop(0, chans // TILE, mixer_cols, 0)

    for here, slot in ((e > 0, e), (e < n_ep - 1, n_ep)):

        @pl.when(here)
        def _():
            for c in range(CHUNKS):
                hop_arrives(slot, c)

        @pl.when(~here)
        def _():
            pin[slot] = jnp.zeros(pin.shape[1:], pin.dtype)

    def combine_cols(c, _):
        at = pl.ds(pl.multiple_of(c * TILE, TILE), TILE)
        part = shd.shape[-1]
        total = dot32(shd[0], sd[0:part, at])
        for lane in range(1, n_tp):
            total += dot32(shd[lane], sd[lane * part : (lane + 1) * part, at])
        for found in (res[e, :, at], pin[e, :, at], pin[n_ep, :, at]):
            total += found.astype(jnp.float32)
        exp_out[:, at] = total.astype(jnp.bfloat16)
        return 0

    lax.fori_loop(0, chans // TILE, combine_cols, 0)

    @pl.when(e < n_ep - 1)
    def _():
        halo_copy().wait_send()

    def drain(j, _):
        def drain_z(d, q):
            @pl.when(goes_right(j))
            def _():
                z_copy(0, d, j, q).wait_send()

            @pl.when(goes_left(j))
            def _():
                z_copy(1, d, j, q).wait_send()

        for q in range(pieces):
            g = j * pieces + q
            drain_z(0, q)
            across(tok_slot(j, q), g, 0, t).wait_send()
            for d in range(1, n_x):

                @pl.when(crosses(j))
                def _():
                    cross(tok_slot(j, q), g, d, t).wait_send()

                @pl.when(at_end(j))
                def _():
                    drain_z(d, q)

                across(tok_slot(j, q), g, d, from_x(d)).wait_send()

        gather_drain(hid_slot(j), first_hidden + j)

        @pl.when(j != e)
        def _():
            for c in range(CHUNKS):
                hop(j, c).wait_send()

        return 0

    lax.fori_loop(0, n_ep, drain, 0)
    for d in range(1, n_ep):
        weights_to(d).wait_send()
    gather_drain(shd_slot, shared_g)
    gather_drain(mixed_slot, mixed_g)


def joined(n_ep, n_tp, *args):
    (og, ig, va, taps, mw, ei, ng, ids, rw, gw, uw, dw, sg, su, sd) = args
    gw, uw, dw, ng = gw[0], uw[0], dw[0], ng[None]
    bf, f32 = jnp.bfloat16, jnp.float32
    rows, chans = og.shape
    lane_rows, width = ei.shape
    n_x = n_tp // CORES
    pieces = lane_rows // PIECE
    sems = n_ep * pieces + n_ep + 2
    big = (og, ig, va, taps, mw, ei, ng, gw, uw, dw, sg, su, sd)
    out = jax.ShapeDtypeStruct((rows, chans), bf)
    vmem = pl.BlockSpec(memory_space=pltpu.VMEM)
    dma = pltpu.SemaphoreType.DMA
    return pl.pallas_call(
        functools.partial(kernel, n_ep, n_tp),
        out_shape=(out, out),
        in_specs=[vmem, vmem] + [pl.BlockSpec(memory_space=pl.ANY)] * len(big),
        out_specs=(vmem, vmem),
        scratch_shapes=[pltpu.VMEM(a.shape, a.dtype) for a in big]
        + [
            pltpu.VMEM((n_ep, n_tp, pieces, PIECE, width), bf),
            pltpu.VMEM((n_ep, n_tp, rows, gw.shape[-1]), bf),
            pltpu.VMEM((n_tp, rows, sg.shape[-1]), bf),
            pltpu.VMEM((n_tp, rows, chans), bf),
            pltpu.VMEM((rows, chans), bf),
            pltpu.VMEM((16, chans), bf),
            pltpu.VMEM((n_ep, rows, chans), bf),
            pltpu.VMEM((n_ep + 1, rows, chans), bf),
            pltpu.VMEM((n_ep, -(-n_ep // 8) * 8, -(-rows // 128) * 128), f32),
            dma((len(big),)),
            dma((2, n_x, n_ep, pieces)),
            dma((n_x, n_ep, pieces)),
            dma((sems, max(1, n_x - 1))),
            dma((sems, max(1, n_x - 1))),
            dma((sems, n_x)),
            dma((sems, n_x)),
            dma((n_ep, CHUNKS)),
            dma((n_ep + 1, CHUNKS)),
            dma((n_ep,)),
            dma((n_ep,)),
            dma((2,)),
        ],
        compiler_params=pltpu.CompilerParams(
            collective_id=0, has_side_effects=True, vmem_limit_bytes=60 * 1024 * 1024
        ),
    )(ids.T, rw.T, *big)


def local(*args):
    n_ep, n_tp = lax.axis_size("ep"), lax.axis_size("tp")
    chans, lane_rows = args[0].shape[1], args[5].shape[0]
    aligned = (
        n_tp % CORES == 0
        and lane_rows % PIECE == 0
        and lane_rows * n_tp == args[0].shape[0]
        and chans % TILE == 0
        and args[0].shape[0] % (16 * CHUNKS) == 0
        and args[9].shape[2] % 128 == 0
        and args[12].shape[1] % 128 == 0
    )
    return joined(n_ep, n_tp, *args) if aligned else plain(*args)


def solution(mesh):
    placed = (
        P(("grp", "ep"), "tp"),
        P(("grp", "ep"), "tp"),
        P(("grp", "ep"), "tp"),
        P(None, "tp"),
        P(None, "tp"),
        P(("grp", "ep", "tp"), None),
        P(),
        P(("grp", "ep"), None),
        P(("grp", "ep"), None),
        P("ep", None, "tp"),
        P("ep", None, "tp"),
        P("ep", None, "tp"),
        P(None, "tp"),
        P(None, "tp"),
        P(None, "tp"),
    )
    return jax.shard_map(
        local,
        mesh=mesh,
        in_specs=placed,
        out_specs=(P(("grp", "ep"), "tp"), P(("grp", "ep"), "tp")),
        check_vma=False,
    )
```

profile of v0, /device:TPU:0, one launch (start us, length us, event | category | flops | bytes accessed | tf_op | source)
XLA Modules:
  0.0 85.4 jit_solution(5186803444216924334)
XLA Ops:
  0.6 81.3 %shard_map.158 = (bf16[192,1024]{1,0:T(8,128)(2,1)}, bf16[192,1024]{1,0:T(8,128)(2,1)}) custom-call(s32[2,192]{1,0:T(2,128)} %bitcast.10, f32[2,192]{1,0:T(2,128)} %bitcast.11, bf16[192,1024]{1,0:T(8,128)(2,1)} %og_h.1, bf16[192,1024]{1,0:T(8,128)(2,1)} %ig_h.1, bf16[192,1024]{1,0:T(8,128)(2,1)} %va_h.1, f32[3,1024]{1,0:T(4,128)} %taps_h.1, ...), custom_call_target="tpu_custom_call" | custom-call | tf_op jit(solution)/shard_map/pallas_call | solution.py:656
  81.9 1.8 %copy.19 = bf16[192,1024]{1,0:T(8,128)(2,1)} copy(bf16[192,1024]{1,0:T(8,128)(2,1)} %get-tuple-element.4) | data formatting | bytes 786432
  83.7 1.8 %copy.20 = bf16[192,1024]{1,0:T(8,128)(2,1)} copy(bf16[192,1024]{1,0:T(8,128)(2,1)} %get-tuple-element.5) | data formatting | bytes 786432
where the time goes:
time: 85.7 us; the launch traced here: 85.4 us
  Pallas kernels  81.3 us (95%)
  local copies, waits for them, and re-layouts  3.53 us (4%)
    pallas_call x1, Pallas kernels, joined(): pl.pallas_call(functools.partial(kernel, n_ep, n_tp), out_shape=(out, out...  81.3 us
    unnamed x2, local copies, waits for them, and re-layouts  3.53 us

commit v1 on v0

--- a/solution.py
+++ b/solution.py
@@ -12,6 +12,7 @@
 TILE = 256
 PIECE = 16
 CHUNKS = 4
+ROLES = 2
 
 norm_floor = 0.5
 
@@ -177,6 +178,7 @@
     halo,
     res,
     pin,
+    acc,
     wts,
     ld,
     z_send,
@@ -288,90 +290,68 @@
     def mixed_slot(lane):
         return mixed.at[lane]
 
-    nearest = jnp.minimum(e, n_ep - 1 - e)
-    left_short = e <= n_ep - 1 - e
-
-    def block_at(k):
-        near = jnp.where(k % 2 == 1, e - (k + 1) // 2, e + k // 2)
-        far = jnp.where(left_short, k, n_ep - 1 - k)
-        return jnp.where(k <= 2 * nearest, near, far)
-
-    def at_end(j):
-        return (j == 0) | (j == n_ep - 1)
-
-    def crosses(j):
-        return (j == e) | ~at_end(j)
+    last = n_ep - 1
+    flipped = e > last - e
+    inner = (e > 0) & (e < last)
+    up = jnp.where(flipped, e - 1, e + 1)
+    down = jnp.clip(jnp.where(flipped, e + 1, e - 1), 0, last)
+
+    def block_at(m):
+        return jnp.where(flipped, last - m, m)
 
     def z_copy(side, d, j, q):
         block = tok.at[j, from_x(d), q]
         return remote(block, block, z_send.at[side, d, j, q], z_recv.at[d, j, q],
-                      jnp.clip(e + 1 - 2 * side, 0, n_ep - 1), t)
-
-    def goes_right(j):
-        return (j <= e) & (e < n_ep - 1)
-
-    def goes_left(j):
-        return (j >= e) & (e > 0)
-
-    def z_onward(d, j, q):
-        @pl.when(goes_right(j))
-        def _():
-            z_copy(0, d, j, q).start()
-
-        @pl.when(goes_left(j))
-        def _():
-            z_copy(1, d, j, q).start()
-
-    def spread(k, q):
-        j = block_at(k)
-        g = j * pieces + q
-
-        @pl.when(k > 0)
-        def _():
-            z_copy(0, 0, j, q).wait_recv()
-
-        z_onward(0, j, q)
-
-        @pl.when(crosses(j))
-        def _():
+                      up if side == 0 else down, t)
+
+    def arrive(m, q, onward=None, crosses=True):
+        j = block_at(m)
+        z_copy(0, 0, j, q).wait_recv()
+        if onward is not None:
+            z_copy(onward, 0, j, q).start()
+        if crosses:
             for d in range(1, n_x):
-                cross(tok_slot(j, q), g, d, t).start()
-
-        across(tok_slot(j, q), g, 0, t).start()
-
-    def forward(k, q):
-        j = block_at(k)
-        g = j * pieces + q
+                cross(tok_slot(j, q), j * pieces + q, d, t).start()
+        across(tok_slot(j, q), j * pieces + q, 0, t).start()
+
+    def arrive_beside(m, q):
+        j = block_at(m)
         for d in range(1, n_x):
-
-            @pl.when(crosses(j))
-            def _():
-                cross(tok_slot(j, q), g, d, from_x(d)).wait_recv()
-
-            @pl.when(~crosses(j))
-            def _():
-                z_copy(0, d, j, q).wait_recv()
-
-            @pl.when(at_end(j))
-            def _():
-                z_onward(d, j, q)
-
-            across(tok_slot(j, q), g, d, from_x(d)).start()
+            z_copy(0, d, j, q).wait_recv()
+            across(tok_slot(j, q), j * pieces + q, d, from_x(d)).start()
+
+    def crossed(m, q, onward=None):
+        j = block_at(m)
+        for d in range(1, n_x):
+            cross(tok_slot(j, q), j * pieces + q, d, from_x(d)).wait_recv()
+            if onward is not None:
+                z_copy(onward, d, j, q).start()
+            across(tok_slot(j, q), j * pieces + q, d, from_x(d)).start()
+
+    def own_onward(side, d, q):
+        z_copy(side, d, e, q).start()
 
     piece = rows // CHUNKS
 
+    def span(c):
+        return pl.ds(pl.multiple_of(c * piece, 16), piece)
+
     def hop(j, c):
-        at = pl.ds(pl.multiple_of(c * piece, 16), piece)
-        after = jnp.clip(jnp.where(j > e, e + 1, e - 1), 0, n_ep - 1)
+        after = jnp.clip(jnp.where(j > e, e + 1, e - 1), 0, last)
         slot = jnp.where((j < e) & (after == j), n_ep, j)
-        return remote(res.at[j, at], pin.at[slot, at], r_send.at[j, c], r_recv.at[slot, c], after, t)
+        return remote(res.at[j, span(c)], pin.at[slot, span(c)],
+                      r_send.at[j, c], r_recv.at[slot, c], after, t)
 
     def hop_arrives(slot, c):
-        at = pl.ds(pl.multiple_of(c * piece, 16), piece)
-        remote(res.at[0, at], pin.at[slot, at], r_send.at[0, c], r_recv.at[slot, c],
-               jnp.clip(e + 1, 0, n_ep - 1), t).wait_recv()
-
-    inner = (e > 0) & (e < n_ep - 1)
+        remote(res.at[0, span(c)], pin.at[slot, span(c)], r_send.at[0, c], r_recv.at[slot, c],
+               jnp.clip(e + 1, 0, last), t).wait_recv()
+
+    def relay(m, c):
+        j = block_at(m)
+        hop_arrives(j, c)
+        total = res[j, span(c), :].astype(jnp.float32) + pin[j, span(c), :].astype(jnp.float32)
+        res[j, span(c), :] = total.astype(jnp.bfloat16)
+        hop(j, c).start()
 
     def weights_to(d):
         return remote(wts.at[e], wts.at[e], w_send.at[d - 1], w_recv.at[e], (e + d) % n_ep, t)
@@ -397,9 +377,21 @@
         return 0
 
     lax.fori_loop(0, pieces, norm_rows, 0)
-    pl.semaphore_wait(barrier, len(greeted))
+    with jax.named_scope("barrier"):
+        pl.semaphore_wait(barrier, len(greeted))
+
     for q in range(pieces):
-        spread(0, q)
+        own_onward(0, 0, q)
+
+        if q < pieces - 1:
+
+            @pl.when(inner)
+            def _():
+                own_onward(1, 0, q)
+
+        for d in range(1, n_x):
+            cross(tok_slot(e, q), e * pieces + q, d, t).start()
+        across(tok_slot(e, q), e * pieces + q, 0, t).start()
 
     place = lax.broadcasted_iota(jnp.int32, (wts.shape[1], rows), 0)
     dense = jnp.zeros(place.shape, jnp.float32)
@@ -424,22 +416,21 @@
 
     def halo_copy():
         return remote(gated.at[pl.ds(rows - 16, 16)], halo, h_sem.at[0], h_sem.at[1],
-                      jnp.minimum(e + 1, n_ep - 1), t)
-
-    @pl.when(e < n_ep - 1)
+                      jnp.minimum(e + 1, last), t)
+
+    @pl.when(e < last)
     def _():
         halo_copy().start()
-
-    loads["og"].wait()
-    loads["taps"].wait()
 
     @pl.when(e == 0)
     def _():
         halo[...] = jnp.zeros_like(halo)
 
-    @pl.when(e > 0)
-    def _():
-        halo_copy().wait_recv()
+    for here, slot in ((e > 0, e), (e < last, n_ep)):
+
+        @pl.when(~here)
+        def _():
+            pin[slot] = jnp.zeros(pin.shape[1:], pin.dtype)
 
     def mix_cols(c, _):
         at = pl.ds(pl.multiple_of(c * 128, 128), 128)
@@ -454,190 +445,279 @@
         mixed[t, :, at] = (og[:, at].astype(jnp.float32) * state).astype(jnp.bfloat16)
         return 0
 
-    lax.fori_loop(0, chans // 128, mix_cols, 0)
-    for name in ("gw", "uw", "sg", "su"):
-        loads[name].wait()
-
-    def leave(k, _):
-        j = block_at(k)
-        gather_forward(hid_slot(j), first_hidden + j)
-        gather_finish(hid_slot(j), first_hidden + j)
+    def end_tokens():
+        for q in range(pieces):
+            if q < pieces - 1:
+                arrive(1, q, crosses=False)
+            crossed(0, q, onward=0)
+        for q in range(pieces):
+            arrive(2, q)
+            if q:
+                crossed(2, q - 1)
+        arrive(3, 0)
+        crossed(2, pieces - 1)
+
+    def end_more():
+        for q in range(1, pieces):
+            arrive(3, q)
+            crossed(3, q - 1)
+        arrive(1, pieces - 1, crosses=False)
+
+    def end_last():
+        crossed(3, pieces - 1)
+
+    def end_beside():
+        for q in range(pieces):
+            arrive_beside(1, q)
+
+    def inner_tokens():
+        for q in range(pieces):
+            arrive(0, q, onward=0, crosses=False)
+            arrive(2, q, onward=1)
+            crossed(1, q)
+        for q in range(pieces):
+            arrive(3, q, onward=1)
+            arrive_beside(0, q)
+            crossed(2, q)
+        own_onward(1, 0, pieces - 1)
+        for d in range(1, n_x):
+            for q in range(pieces):
+                own_onward(1, d, q)
+
+    def inner_more():
+        for q in range(pieces):
+            crossed(3, q)
+
+    def relays(m, chunks):
+        for c in chunks:
+            relay(m, c)
+
+    half = CHUNKS // 2
+    early, late = range(half), range(half, CHUNKS)
+    steps = 7
+    gates = ((2, 3, 1, 0), (2, 0, 3, 1))
+    downs = ((-1, 2, -1, 3, 1, 0, -1), (-1, -1, -1, 2, 3, 0, 1))
+    before_down = (
+        {1: end_more},
+        {5: lambda: relays(2, early), 6: lambda: relays(2, late)},
+    )
+    before_gate = (
+        {0: end_tokens, 1: end_last, 2: end_beside},
+        {0: inner_tokens, 2: inner_more},
+    )
+
+    def table(pair, s):
+        found = jnp.int32(-1)
+        for k, (end_m, inner_m) in enumerate(zip(*pair)):
+            found = jnp.where(s == k, jnp.where(inner, inner_m, end_m), found)
+        return found
+
+    def due(pair, s):
+        for part, here in zip(pair, (~inner, inner)):
+            for k, what in part.items():
+
+                @pl.when(here & (s == k))
+                def _():
+                    what()
+
+    def down_block(j):
         part = hid.shape[-1]
-
-        @pl.when(j != e)
-        def _():
-            remote(wts.at[e], wts.at[j], w_send.at[0], w_recv.at[j], j, t).wait_recv()
-
-        weight = weight_column(j)
-        for c in range(chans // TILE):
-            at = slice(c * TILE, (c + 1) * TILE)
-            total = dot32(hid[j, 0], dw[0:part, at])
-            for lane in range(1, n_tp):
-                total += dot32(hid[j, lane], dw[lane * part : (lane + 1) * part, at])
-            res[j, :, at] = (weight * total).astype(jnp.bfloat16)
+        with jax.named_scope("hid_wait"):
+            gather_forward(hid_slot(j), first_hidden + j)
+            gather_finish(hid_slot(j), first_hidden + j)
+
+            @pl.when(j != e)
+            def _():
+                remote(wts.at[e], wts.at[j], w_send.at[0], w_recv.at[j], j, t).wait_recv()
+
+        with jax.named_scope("down"):
+            weight = weight_column(j)
+            for c in range(chans // TILE):
+                at = slice(c * TILE, (c + 1) * TILE)
+                total = dot32(hid[j, 0], dw[0:part, at])
+                for lane in range(1, n_tp):
+                    total += dot32(hid[j, lane], dw[lane * part : (lane + 1) * part, at])
+                res[j, :, at] = (weight * total).astype(jnp.bfloat16)
 
         @pl.when((j != e) & ~inner)
         def _():
             for c in range(CHUNKS):
                 hop(j, c).start()
+
+    def gate_block(j, s):
+        with jax.named_scope("gate_wait"):
+            for q in range(pieces):
+                gather_finish(tok_slot(j, q), j * pieces + q)
+
+            @pl.when(s == 0)
+            def _():
+                for name in ("gw", "uw", "sg", "su", "dw"):
+                    loads[name].wait()
+
+        with jax.named_scope("gate"):
+            block = tok[j].reshape(rows, width)
+            hid[j, t] = silu_product(dot32(block, gw[...]), dot32(block, uw[...]))
+            gather_start(hid_slot(j), first_hidden + j)
+
+    def step(s, _):
+        with jax.named_scope("pre_down"):
+            due(before_down, s)
+        down_m = table(downs, s)
+
+        @pl.when(down_m >= 0)
+        def _():
+            down_block(block_at(down_m))
+
+        with jax.named_scope("pre_gate"):
+            due(before_gate, s)
+
+        @pl.when(s < n_ep)
+        def _():
+            gate_block(block_at(table(gates, s)), s)
+
+        @pl.when(s == n_ep - 1)
+        def _():
+            with jax.named_scope("shared"):
+                block = tok[e].reshape(rows, width)
+                shd[t] = silu_product(dot32(block, sg[...]), dot32(block, su[...]))
+                gather_start(shd_slot, shared_g)
+            with jax.named_scope("mix"):
+                loads["og"].wait()
+                loads["taps"].wait()
+
+                @pl.when(e > 0)
+                def _():
+                    halo_copy().wait_recv()
+
+                lax.fori_loop(0, chans // 128, mix_cols, 0)
+                gather_start(mixed_slot, mixed_g)
+
         return 0
 
-    def meet(k):
-        j = block_at(k)
-        for q in range(pieces):
-            gather_finish(tok_slot(j, q), j * pieces + q)
-        block = tok[j].reshape(rows, width)
-        hid[j, t] = silu_product(dot32(block, gw[...]), dot32(block, uw[...]))
-        gather_start(hid_slot(j), first_hidden + j)
-
-        @pl.when(k == 0)
+    lax.fori_loop(0, steps, step, 0)
+
+    with jax.named_scope("acc"):
+        gather_forward(shd_slot, shared_g)
+
+        @pl.when(inner)
         def _():
-            block = tok[e].reshape(rows, width)
-            shd[t] = silu_product(dot32(block, sg[...]), dot32(block, su[...]))
-            gather_start(shd_slot, shared_g)
-            loads["dw"].wait()
-
-        @pl.when(k == n_ep - 1)
+            relay(3, 0)
+
+        loads["sd"].wait()
+        gather_finish(shd_slot, shared_g)
+
+        def shared_cols(c, _):
+            at = pl.ds(pl.multiple_of(c * TILE, TILE), TILE)
+            part = shd.shape[-1]
+            total = dot32(shd[0], sd[0:part, at])
+            for lane in range(1, n_tp):
+                total += dot32(shd[lane], sd[lane * part : (lane + 1) * part, at])
+            acc[:, at] = total + res[e, :, at].astype(jnp.float32)
+            return 0
+
+        lax.fori_loop(0, chans // TILE, shared_cols, 0)
+
+    with jax.named_scope("mixed_wait"):
+        @pl.when(inner)
         def _():
-            gather_start(mixed_slot, mixed_g)
-
-    def step(s, _):
-        for q in range(pieces):
-
-            @pl.when(s + 1 < n_ep)
-            def _():
-                spread(s + 1, q)
-
-            @pl.when(s < n_ep)
-            def _():
-                forward(s, q)
-
-        @pl.when(~inner)
-        def _():
-            lax.fori_loop(jnp.maximum(s - 1, 0), s, leave, 0)
-
-        k = jnp.where(inner, s - 1, s)
-
-        @pl.when((k >= 0) & (k < n_ep))
-        def _():
-            meet(k)
-
-        @pl.when(inner & (s == n_ep))
-        def _():
-            lax.fori_loop(0, n_ep, leave, 0)
-
+            relay(3, 1)
+
+        loads["mw"].wait()
+        gather_forward(mixed_slot, mixed_g)
+        gather_finish(mixed_slot, mixed_g)
+
+    tiles = chans // TILE
+    rest = [(3, c) for c in range(2, CHUNKS)]
+    back = [(0, c) for c in range(CHUNKS)]
+    waves = []
+    while rest or back:
+        waves.append([pop.pop(0) for pop in (rest, back) if pop])
+
+    def mixer_cols(c, _):
+        with jax.named_scope("relay"):
+            for k in range(tiles):
+                share = [one for w in range(k, len(waves), tiles) for one in waves[w]]
+
+                @pl.when(inner & (c == k))
+                def _():
+                    for m, chunk in share:
+                        relay(m, chunk)
+
+        with jax.named_scope("mixer"):
+            at = pl.ds(pl.multiple_of(c * TILE, TILE), TILE)
+            total = dot32(mixed[0], mw[0:chans, at])
+            for lane in range(1, n_tp):
+                total += dot32(mixed[lane], mw[lane * chans : (lane + 1) * chans, at])
+            mix_out[:, at] = total.astype(jnp.bfloat16)
         return 0
 
-    lax.fori_loop(0, n_ep + 1, step, 0)
-
-    gather_forward(shd_slot, shared_g)
-
-    for phase in range(2):
-        right = left_short if phase == 0 else ~left_short
-
-        def relay(d, _):
-            j = jnp.where(right, e + d, e - d)
-
-            @pl.when(inner & (j >= 0) & (j < n_ep))
-            def _():
-                def relay_piece(c, _):
-                    at = pl.ds(pl.multiple_of(c * piece, 16), piece)
-                    hop_arrives(j, c)
-                    total = res[j, at, :].astype(jnp.float32) + pin[j, at, :].astype(jnp.float32)
-                    res[j, at, :] = total.astype(jnp.bfloat16)
-                    hop(j, c).start()
-                    return 0
-
-                lax.fori_loop(0, CHUNKS, relay_piece, 0)
-
-            return 0
-
-        lax.fori_loop(1, n_ep, relay, 0)
-
-    gather_forward(mixed_slot, mixed_g)
-    gather_finish(shd_slot, shared_g)
-    loads["sd"].wait()
-    loads["mw"].wait()
-    gather_finish(mixed_slot, mixed_g)
-
-    def mixer_cols(c, _):
-        at = pl.ds(pl.multiple_of(c * TILE, TILE), TILE)
-        total = dot32(mixed[0], mw[0:chans, at])
-        for lane in range(1, n_tp):
-            total += dot32(mixed[lane], mw[lane * chans : (lane + 1) * chans, at])
-        mix_out[:, at] = total.astype(jnp.bfloat16)
+    lax.fori_loop(0, tiles, mixer_cols, 0)
+
+    def combine(c, _):
+        with jax.named_scope("final_wait"):
+            for here, slot in ((e > 0, e), (e < last, n_ep)):
+
+                @pl.when(here)
+                def _():
+                    hop_arrives(slot, c)
+
+        total = acc[span(c), :]
+        for found in (pin[e, span(c), :], pin[n_ep, span(c), :]):
+            total += found.astype(jnp.float32)
+        exp_out[span(c), :] = total.astype(jnp.bfloat16)
         return 0
 
-    lax.fori_loop(0, chans // TILE, mixer_cols, 0)
-
-    for here, slot in ((e > 0, e), (e < n_ep - 1, n_ep)):
-
-        @pl.when(here)
-        def _():
-            for c in range(CHUNKS):
-                hop_arrives(slot, c)
-
-        @pl.when(~here)
-        def _():
-            pin[slot] = jnp.zeros(pin.shape[1:], pin.dtype)
-
-    def combine_cols(c, _):
-        at = pl.ds(pl.multiple_of(c * TILE, TILE), TILE)
-        part = shd.shape[-1]
-        total = dot32(shd[0], sd[0:part, at])
-        for lane in range(1, n_tp):
-            total += dot32(shd[lane], sd[lane * part : (lane + 1) * part, at])
-        for found in (res[e, :, at], pin[e, :, at], pin[n_ep, :, at]):
-            total += found.astype(jnp.float32)
-        exp_out[:, at] = total.astype(jnp.bfloat16)
-        return 0
-
-    lax.fori_loop(0, chans // TILE, combine_cols, 0)
-
-    @pl.when(e < n_ep - 1)
+    lax.fori_loop(0, CHUNKS, combine, 0)
+
+    @pl.when(e < last)
     def _():
         halo_copy().wait_send()
 
-    def drain(j, _):
-        def drain_z(d, q):
-            @pl.when(goes_right(j))
+    with jax.named_scope("drain"):
+        for q in range(pieces):
+            for side, d, m in ((0, 0, None),):
+                z_copy(side, d, e, q).wait_send()
+
+            @pl.when(~inner)
             def _():
-                z_copy(0, d, j, q).wait_send()
-
-            @pl.when(goes_left(j))
+                for d in range(1, n_x):
+                    z_copy(0, d, e, q).wait_send()
+
+            @pl.when(inner)
             def _():
-                z_copy(1, d, j, q).wait_send()
-
-        for q in range(pieces):
-            g = j * pieces + q
-            drain_z(0, q)
-            across(tok_slot(j, q), g, 0, t).wait_send()
-            for d in range(1, n_x):
-
-                @pl.when(crosses(j))
-                def _():
-                    cross(tok_slot(j, q), g, d, t).wait_send()
-
-                @pl.when(at_end(j))
-                def _():
-                    drain_z(d, q)
-
-                across(tok_slot(j, q), g, d, from_x(d)).wait_send()
-
-        gather_drain(hid_slot(j), first_hidden + j)
-
-        @pl.when(j != e)
-        def _():
-            for c in range(CHUNKS):
-                hop(j, c).wait_send()
-
-        return 0
-
-    lax.fori_loop(0, n_ep, drain, 0)
-    for d in range(1, n_ep):
-        weights_to(d).wait_send()
-    gather_drain(shd_slot, shared_g)
-    gather_drain(mixed_slot, mixed_g)
+                for d in range(n_x):
+                    z_copy(1, d, e, q).wait_send()
+                z_copy(0, 0, block_at(0), q).wait_send()
+                for m in (2, 3):
+                    z_copy(1, 0, block_at(m), q).wait_send()
+
+        beside = jnp.where(inner, block_at(0), block_at(1))
+
+        def drain(j, _):
+            for q in range(pieces):
+                g = j * pieces + q
+                across(tok_slot(j, q), g, 0, t).wait_send()
+                for d in range(1, n_x):
+
+                    @pl.when(j != beside)
+                    def _():
+                        cross(tok_slot(j, q), g, d, t).wait_send()
+
+                    across(tok_slot(j, q), g, d, from_x(d)).wait_send()
+            gather_drain(hid_slot(j), first_hidden + j)
+
+            @pl.when(j != e)
+            def _():
+                for c in range(CHUNKS):
+                    hop(j, c).wait_send()
+
+            return 0
+
+        lax.fori_loop(0, n_ep, drain, 0)
+        for d in range(1, n_ep):
+            weights_to(d).wait_send()
+        gather_drain(shd_slot, shared_g)
+        gather_drain(mixed_slot, mixed_g)
 
 
 def joined(n_ep, n_tp, *args):
@@ -668,6 +748,7 @@
             pltpu.VMEM((16, chans), bf),
             pltpu.VMEM((n_ep, rows, chans), bf),
             pltpu.VMEM((n_ep + 1, rows, chans), bf),
+            pltpu.VMEM((rows, chans), f32),
             pltpu.VMEM((n_ep, -(-n_ep // 8) * 8, -(-rows // 128) * 128), f32),
             dma((len(big),)),
             dma((2, n_x, n_ep, pieces)),
@@ -693,6 +774,7 @@
     chans, lane_rows = args[0].shape[1], args[5].shape[0]
     aligned = (
         n_tp % CORES == 0
+        and n_ep == 2 * ROLES
         and lane_rows % PIECE == 0
         and lane_rows * n_tp == args[0].shape[0]
         and chans % TILE == 0

time: 85.7 us -> 73.8 us (0.86)
  Pallas kernels: 81.3 us -> 69.4 us
    pallas_call x1, Pallas kernels: 81.3 us -> 69.4 us  [joined(): pl.pallas_call(functools.partial(kernel, n_ep, n_tp), out_shape=(out, out...]
where the time goes in v1:
time: 73.8 us; the launch traced here: 73.6 us
  Pallas kernels  69.4 us (94%)
  local copies, waits for them, and re-layouts  3.53 us (5%)
    pallas_call x1, Pallas kernels, joined(): pl.pallas_call(functools.partial(kernel, n_ep, n_tp), out_shape=(out, out...  69.4 us
    unnamed x2, local copies, waits for them, and re-layouts  3.53 us

profile of v1, /device:TPU:0, one launch (start us, length us, event | category | flops | bytes accessed | tf_op | source)
XLA Modules:
  0.0 73.6 jit_solution(3141637640294858973)
XLA Ops:
  0.6 69.4 %shard_map.158 = (bf16[192,1024]{1,0:T(8,128)(2,1)}, bf16[192,1024]{1,0:T(8,128)(2,1)}) custom-call(s32[2,192]{1,0:T(2,128)} %bitcast.10, f32[2,192]{1,0:T(2,128)} %bitcast.11, bf16[192,1024]{1,0:T(8,128)(2,1)} %og_h.1, bf16[192,1024]{1,0:T(8,128)(2,1)} %ig_h.1, bf16[192,1024]{1,0:T(8,128)(2,1)} %va_h.1, f32[3,1024]{1,0:T(4,128)} %taps_h.1, ...), custom_call_target="tpu_custom_call" | custom-call | tf_op jit(solution)/shard_map/pallas_call | solution.py:736
  70.0 1.8 %copy.19 = bf16[192,1024]{1,0:T(8,128)(2,1)} copy(bf16[192,1024]{1,0:T(8,128)(2,1)} %get-tuple-element.4) | data formatting | bytes 786432
  71.8 1.8 %copy.20 = bf16[192,1024]{1,0:T(8,128)(2,1)} copy(bf16[192,1024]{1,0:T(8,128)(2,1)} %get-tuple-element.5) | data formatting | bytes 786432

commit v2 on v1

v2 whole, which is shorter than its diff:
```python
import functools

import jax
import jax.numpy as jnp
from jax import lax
from jax.experimental import pallas as pl
from jax.experimental.pallas import tpu as pltpu
from jax.sharding import PartitionSpec as P

MESH = pl.DeviceIdType.MESH
CORES = 2
TILE = 256
PIECE = 16
CHUNKS = 4
ROLES = 2
STEPS = 3
SUB = 1

END_PLAN = dict(
    gates=("20", "21", "22", "30", "31", "32", "10", "11", "12", "--", "--", "--"),
    downs=("--", "--", "--", "20", "21", "22", "30", "31", "32", "10", "11", "12"),
    before_down={
    },
    before_gate={
        0: ("N10", "O00", "N11", "O01", "X00", "M00", "O02", "A20", "D00", "E00", "A21", "S00", "B20"),
        1: ("A22", "W00", "B21"),
        2: ("A30", "B22", "A31", "H20"),
        3: ("A32", "B30", "H21"),
        4: ("N12", "B31", "H22"),
        5: ("Z10", "B32", "H30"),
        6: ("H31",),
        7: ("Z11", "H32"),
        8: ("Z12", "H10"),
        9: ("H11",),
        10: ("H12",),
    },
    after_gate={
        5: ("M01",),
        6: ("M02",),
        7: ("M03",),
        8: ("K00",),
    },
)
INNER_PLAN = dict(
    gates=("20", "00", "30", "--", "--", "--", "--"),
    downs=("--", "--", "--", "20", "00", "30", "10"),
    before_down={
        3: ("T20",),
        4: ("R20", "R21", "T00"),
        5: ("T30",),
        6: ("R22", "T10"),
    },
    before_gate={
        0: ("P00", "P01", "P02", "X00", "W00", "D00", "E00", "Q00", "S00", "Q01", "Q02", "L00"),
        2: ("B30", "B31", "B32"),
        3: ("M00", "K00", "M01", "M02", "M03"),
    },
    after_gate={
    },
)
AFTER_STEPS = ("30", "31", "00", "32")
BESIDE_MIXER = {0: ("R01",), 1: ("R02",)}

norm_floor = 0.5


def shifted(value, axis, steps):
    count = lax.axis_size(axis)
    leading, last = (max(0, -steps), min(count, count - steps))
    return lax.ppermute(value, axis, [(source, source + steps) for source in range(leading, last)])


def layer_norm(tokens, norm_gain):
    widened = tokens.astype(jnp.float32)
    centred = widened - jnp.mean(widened, axis=-1, keepdims=True)
    spread = jnp.mean(centred * centred, axis=-1, keepdims=True)
    return (centred * lax.rsqrt(spread + norm_floor) * norm_gain).astype(jnp.bfloat16)


def expert_hidden(inputs, gate_part, up_part):
    gate_value = jnp.dot(inputs, gate_part, preferred_element_type=jnp.float32)
    up_value = jnp.dot(inputs, up_part, preferred_element_type=jnp.float32)
    return (jax.nn.silu(gate_value) * up_value).astype(jnp.bfloat16)


def slot_ranks(route_ids, experts, lanes):
    tok_count, top_count = route_ids.shape
    grouped = route_ids.reshape(lanes, tok_count // lanes * top_count)
    onehot = (grouped[:, :, None] == jnp.arange(experts, dtype=jnp.int32)[None, None, :]).astype(
        jnp.int32
    )
    before = jnp.cumsum(onehot, axis=1) - onehot
    return jnp.sum(before * onehot, axis=2).reshape(tok_count, top_count)


def plain(
    out_gate,
    in_gate,
    values,
    conv_taps,
    mixer_weight,
    expert_input,
    norm_gain,
    route_ids,
    route_weights,
    gate_weight,
    up_weight,
    down_weight,
    shared_gate,
    shared_up,
    shared_down,
):
    experts = lax.axis_size("ep")
    lanes = lax.axis_size("tp")
    lane_rows = expert_input.shape[0]
    width = expert_input.shape[1]
    tok_count, top_count = route_ids.shape
    capacity = (2 * lane_rows * top_count + experts - 1) // experts
    gated_values = (in_gate.astype(jnp.float32) * values.astype(jnp.float32)).astype(jnp.bfloat16)
    previous = shifted(gated_values[-2:], "ep", 1)
    extended = jnp.concatenate([previous, gated_values], axis=0).astype(jnp.float32)
    conv_state = (
        conv_taps[0] * extended[:-2] + conv_taps[1] * extended[1:-1] + conv_taps[2] * extended[2:]
    )
    mixed_rows = (out_gate.astype(jnp.float32) * conv_state).astype(jnp.bfloat16)
    normed_own = layer_norm(expert_input, norm_gain)
    mixed_whole, normed_rows = (
        lax.all_gather(mixed_rows, "tp", axis=1, tiled=True),
        lax.all_gather(normed_own, "tp", axis=0, tiled=True),
    )
    mixer_output = jnp.dot(mixed_whole, mixer_weight, preferred_element_type=jnp.float32).astype(
        jnp.bfloat16
    )
    shared_part = expert_hidden(normed_rows, shared_gate, shared_up)
    slot_index = slot_ranks(route_ids, experts, lanes)
    lane_of_row = (jnp.arange(tok_count, dtype=jnp.int32) // lane_rows)[:, None]
    positions = (route_ids * lanes + lane_of_row) * capacity + slot_index
    lane_index = lax.axis_index("tp")
    lane_ids = lax.dynamic_slice_in_dim(route_ids, lane_index * lane_rows, lane_rows, 0)
    lane_slots = lax.dynamic_slice_in_dim(slot_index, lane_index * lane_rows, lane_rows, 0)
    lane_places = lane_ids * capacity + lane_slots
    local_rows = jnp.broadcast_to(jnp.arange(lane_rows, dtype=jnp.int32)[:, None], lane_ids.shape)
    owners = jnp.full((experts * capacity,), lane_rows, jnp.int32)
    owners = owners.at[lane_places.reshape(-1)].set(local_rows.reshape(-1))
    outgoing = jnp.take(normed_own, owners, axis=0, mode="fill", fill_value=0)
    arrived = lax.all_to_all(
        outgoing.reshape(experts, capacity, width), "ep", split_axis=0, concat_axis=0, tiled=True
    )
    segment = lax.all_gather(arrived[None], "tp", axis=0, tiled=True)
    hidden_rows = expert_hidden(segment.reshape(-1, width), gate_weight[0], up_weight[0])
    spread_hidden = hidden_rows.reshape(segment.shape[:-1] + (hidden_rows.shape[-1],))
    routed_hidden = jnp.swapaxes(spread_hidden, 0, 1).reshape(-1, spread_hidden.shape[-1])
    routed_whole, shared_whole = (
        lax.all_gather(routed_hidden, "tp", axis=1, tiled=True),
        lax.all_gather(shared_part, "tp", axis=1, tiled=True),
    )
    routed_result = jnp.dot(
        routed_whole, down_weight[0], preferred_element_type=jnp.float32
    ).astype(jnp.bfloat16)
    out_cols = routed_result.shape[-1]
    returned = lax.all_to_all(
        routed_result.reshape(experts, lanes * capacity, out_cols),
        "ep",
        split_axis=0,
        concat_axis=0,
        tiled=True,
    )
    shared_result = jnp.dot(shared_whole, shared_down, preferred_element_type=jnp.float32)
    picked = jnp.take(
        returned.reshape(experts * lanes * capacity, out_cols), positions.reshape(-1), axis=0
    )
    picked = picked.astype(jnp.float32).reshape(tok_count, top_count, out_cols)
    expert_output = (shared_result + jnp.sum(route_weights[:, :, None] * picked, axis=1)).astype(
        jnp.bfloat16
    )
    return (mixer_output, expert_output)


def silu_product(gate_value, up_value):
    return (gate_value * (1.0 / (1.0 + jnp.exp(-gate_value))) * up_value).astype(jnp.bfloat16)


def dot32(left, right):
    return jnp.dot(left, right, preferred_element_type=jnp.float32)


def kernel(
    n_ep,
    n_tp,
    ids_h,
    rw_h,
    og_h,
    ig_h,
    va_h,
    taps_h,
    mw_h,
    ei_h,
    ng_h,
    gw_h,
    uw_h,
    dw_h,
    sg_h,
    su_h,
    sd_h,
    mix_out,
    exp_out,
    og,
    ig,
    va,
    taps,
    mw,
    ei,
    ng,
    gw,
    uw,
    dw,
    sg,
    su,
    sd,
    ids,
    rw,
    tok,
    hid,
    shd,
    mixed,
    gated,
    halo,
    res,
    pin,
    acc,
    wcol,
    wts,
    ld,
    z_send,
    z_recv,
    x_send,
    x_recv,
    p_send,
    p_recv,
    r_send,
    r_recv,
    w_send,
    w_recv,
    h_sem,
):
    e = lax.axis_index("ep")
    t = lax.axis_index("tp")
    n_x = n_tp // CORES
    partner = t + 1 - 2 * (t % CORES)
    lane_rows, width = ei.shape
    rows, chans = og.shape

    pieces = lane_rows // PIECE
    loads = {}

    def load(name, src, dst):
        loads[name] = pltpu.make_async_copy(src, dst, ld.at[len(loads)])
        loads[name].start()

    for q in range(pieces):
        load(f"ei{q}", ei_h.at[pl.ds(q * PIECE, PIECE)], ei.at[pl.ds(q * PIECE, PIECE)])
    load("ng", ng_h, ng)

    barrier = pltpu.get_barrier_semaphore()
    greeted = [{"ep": (e + d) % n_ep, "tp": t} for d in range(1, n_ep)]
    greeted += [{"ep": e, "tp": (t + CORES * d) % n_tp} for d in range(1, n_x)]
    greeted += [{"ep": e, "tp": partner}]
    for peer in greeted:
        pl.semaphore_signal(barrier, inc=1, device_id=peer, device_id_type=MESH)

    for name, src, dst in (
        ("ids", ids_h, ids),
        ("rw", rw_h, rw),
        ("ig", ig_h, ig),
        ("va", va_h, va),
    ):
        load(name, src, dst)

    def remote(src, dst, send, recv, ep, tp):
        return pltpu.make_async_remote_copy(
            src_ref=src,
            dst_ref=dst,
            send_sem=send,
            recv_sem=recv,
            device_id={"ep": ep, "tp": tp},
            device_id_type=MESH,
        )

    def cross(slot, g, d, lane):
        return remote(
            slot(lane), slot(lane), x_send.at[slot.kind], x_recv.at[g, d - 1],
            e, (t + CORES * d) % n_tp,
        )

    def across(slot, g, d, lane):
        return remote(slot(lane), slot(lane), p_send.at[slot.kind], p_recv.at[g, d], e, partner)

    def from_x(d):
        return (t + n_tp - CORES * d) % n_tp

    def from_partner(d):
        return (partner + n_tp - CORES * d) % n_tp

    def gather_start(slot, g):
        for d in range(1, n_x):
            cross(slot, g, d, t).start()
        across(slot, g, 0, t).start()

    def gather_forward(slot, g):
        for d in range(1, n_x):
            cross(slot, g, d, from_x(d)).wait_recv()
            across(slot, g, d, from_x(d)).start()

    def gather_finish(slot, g):
        for d in range(n_x):
            across(slot, g, d, from_partner(d)).wait_recv()

    first_hidden = n_ep * pieces
    shared_g = 2 * first_hidden
    mixed_g = shared_g + 1
    strip = rows // CHUNKS

    class Slot:
        def __init__(self, kind, at):
            self.kind, self.at = kind, at

        def __call__(self, lane):
            return self.at(lane)

    def tok_slot(j, q):
        return Slot(0, lambda lane: tok.at[j, lane, q])

    def hid_slot(j, q):
        return Slot(1, lambda lane: hid.at[j, q, lane])

    def hid_g(j, q):
        return first_hidden + j * pieces + q

    shd_slot = Slot(2, lambda lane: shd.at[lane])

    def mixed_slot(k):
        return Slot(3, lambda lane: mixed.at[lane, pl.ds(k * strip, strip)])

    last = n_ep - 1
    flipped = e > last - e
    inner = (e > 0) & (e < last)
    up = jnp.where(flipped, e - 1, e + 1)
    down = jnp.clip(jnp.where(flipped, e + 1, e - 1), 0, last)

    def block_at(m):
        return jnp.where(flipped, last - m, m)

    def z_copy(side, d, j, q, own=0):
        block = tok.at[j, from_x(d), q]
        return remote(block, block, z_send.at[side + own * side], z_recv.at[d, j, q],
                      up if side == 0 else down, t)

    def arrive(m, q, onward=None, crosses=True):
        j = block_at(m)
        z_copy(0, 0, j, q).wait_recv()
        if onward is not None:
            z_copy(onward, 0, j, q).start()
        if crosses:
            for d in range(1, n_x):
                cross(tok_slot(j, q), j * pieces + q, d, t).start()
        across(tok_slot(j, q), j * pieces + q, 0, t).start()

    def arrive_beside(m, q):
        j = block_at(m)
        for d in range(1, n_x):
            z_copy(0, d, j, q).wait_recv()
            across(tok_slot(j, q), j * pieces + q, d, from_x(d)).start()

    def crossed(m, q, onward=None):
        j = block_at(m)
        for d in range(1, n_x):
            cross(tok_slot(j, q), j * pieces + q, d, from_x(d)).wait_recv()
            if onward is not None:
                z_copy(onward, d, j, q).start()
            across(tok_slot(j, q), j * pieces + q, d, from_x(d)).start()

    def own_onward(side, d, q):
        z_copy(side, d, e, q, own=1).start()

    part_rows = n_tp * PIECE
    halves = part_rows // SUB

    def half(h):
        return pl.ds(h * halves, halves)

    def hop(j, q, h):
        after = jnp.clip(jnp.where(j > e, e + 1, e - 1), 0, last)
        slot = jnp.where((j < e) & (after == j), n_ep, j)
        return remote(res.at[j, q, half(h)], pin.at[slot, q, half(h)],
                      r_send.at[0], r_recv.at[slot, q, h], after, t)

    def hop_arrives(slot, q, h):
        remote(res.at[0, q, half(h)], pin.at[slot, q, half(h)], r_send.at[0],
               r_recv.at[slot, q, h], jnp.clip(e + 1, 0, last), t).wait_recv()

    def relay(m, q):
        j = block_at(m)
        with jax.named_scope(f"relay{m}{q}"):
            for h in range(SUB):
                hop_arrives(j, q, h)
                total = res[j, q, half(h)].astype(jnp.float32) + pin[j, q, half(h)].astype(jnp.float32)
                res[j, q, half(h)] = total.astype(jnp.bfloat16)
                hop(j, q, h).start()

    def weights_to(d):
        return remote(wts.at[e], wts.at[e], w_send.at[0], w_recv.at[e], (e + d) % n_ep, t)

    def weight_column(j):
        held = wts[j]
        mine = jnp.where(lax.broadcasted_iota(jnp.int32, held.shape, 0) == e, held, 0.0)
        line = jnp.sum(mine, axis=0, keepdims=True)
        shape = (rows, held.shape[1])
        same = lax.broadcasted_iota(jnp.int32, shape, 0) == lax.broadcasted_iota(jnp.int32, shape, 1)
        return jnp.sum(jnp.where(same, line, 0.0), axis=1, keepdims=True)

    loads["ng"].wait()
    for q in range(pieces):
        loads[f"ei{q}"].wait()
        widened = ei[q * PIECE : (q + 1) * PIECE, :].astype(jnp.float32)
        centred = widened - jnp.mean(widened, axis=-1, keepdims=True)
        spread_of = jnp.mean(centred * centred, axis=-1, keepdims=True)
        normed = centred * lax.rsqrt(spread_of + norm_floor) * ng[...]
        tok[e, t, q] = normed.astype(jnp.bfloat16)

    for name, src, dst in (
        ("gw", gw_h, gw),
        ("uw", uw_h, uw),
        ("og", og_h, og),
        ("taps", taps_h, taps),
        ("sg", sg_h, sg),
        ("su", su_h, su),
        ("dw", dw_h, dw),
        ("sd", sd_h, sd),
        ("mw", mw_h, mw),
    ):
        load(name, src, dst)

    with jax.named_scope("barrier"):
        pl.semaphore_wait(barrier, len(greeted))

    for q in range(pieces):
        own_onward(0, 0, q)

        if q < pieces - 1:

            @pl.when(inner)
            def _():
                own_onward(1, 0, q)

        for d in range(1, n_x):
            cross(tok_slot(e, q), e * pieces + q, d, t).start()
        across(tok_slot(e, q), e * pieces + q, 0, t).start()

    loads["ids"].wait()
    loads["rw"].wait()
    place = lax.broadcasted_iota(jnp.int32, (wts.shape[1], rows), 0)
    dense = jnp.zeros(place.shape, jnp.float32)
    for k in range(ids.shape[0]):
        dense += jnp.where(ids[k : k + 1, :] == place, rw[k : k + 1, :], 0.0)
    wts[e] = jnp.zeros(wts.shape[1:], jnp.float32)
    wts[e, :, 0:rows] = dense
    for d in range(1, n_ep):
        weights_to(d).start()

    loads["ig"].wait()
    loads["va"].wait()

    def gate_cols(c, _):
        at = pl.ds(pl.multiple_of(c * 128, 128), 128)
        gated[:, at] = (ig[:, at].astype(jnp.float32) * va[:, at].astype(jnp.float32)).astype(
            jnp.bfloat16
        )
        return 0

    lax.fori_loop(0, chans // 128, gate_cols, 0)

    def halo_copy():
        return remote(gated.at[pl.ds(rows - 16, 16)], halo, h_sem.at[0], h_sem.at[1],
                      jnp.minimum(e + 1, last), t)

    @pl.when(e < last)
    def _():
        halo_copy().start()

    @pl.when(e == 0)
    def _():
        halo[...] = jnp.zeros_like(halo)

    for here, slot in ((e > 0, e), (e < last, n_ep)):

        @pl.when(~here)
        def _():
            pin[slot] = jnp.zeros(pin.shape[1:], pin.dtype)

    def mix_cols(c, _):
        at = pl.ds(pl.multiple_of(c * 128, 128), 128)
        now = gated[:, at].astype(jnp.float32)
        before = halo[:, at].astype(jnp.float32)
        place = lax.broadcasted_iota(jnp.int32, now.shape, 0)
        one = jnp.where(place == 0, before[15:16], pltpu.roll(now, 1, 0))
        two = jnp.where(
            place == 0, before[14:15], jnp.where(place == 1, before[15:16], pltpu.roll(now, 2, 0))
        )
        state = taps[0:1, at] * two + taps[1:2, at] * one + taps[2:3, at] * now
        mixed[t, :, at] = (og[:, at].astype(jnp.float32) * state).astype(jnp.bfloat16)
        return 0

    def mix():
        with jax.named_scope("mix"):
            loads["og"].wait()
            loads["taps"].wait()

            @pl.when(e > 0)
            def _():
                halo_copy().wait_recv()

            lax.fori_loop(0, chans // 128, mix_cols, 0)

    def weigh():
        def column(j, _):
            @pl.when(j != e)
            def _():
                remote(wts.at[e], wts.at[j], w_send.at[0], w_recv.at[j], j, t).wait_recv()

            spread_out = jnp.broadcast_to(weight_column(j), (rows, wcol.shape[-1]))
            spread_out = spread_out.reshape(n_tp, pieces, PIECE, wcol.shape[-1])
            for q in range(pieces):
                wcol[j, q] = spread_out[:, q].reshape(part_rows, wcol.shape[-1])
            return 0

        with jax.named_scope("weigh"):
            lax.fori_loop(0, n_ep, column, 0)

    def own_late():
        own_onward(1, 0, pieces - 1)
        for d in range(1, n_x):
            for q in range(pieces):
                own_onward(1, d, q)

    def own_crossed(q):
        crossed(0, q, onward=0)

    def inner_pair(q):
        arrive(0, q, onward=0, crosses=False)
        arrive(2, q, onward=1)
        crossed(1, q)

    def inner_far(q):
        arrive(3, q, onward=1)
        arrive_beside(0, q)
        crossed(2, q)

    def passed(m, q):
        j = block_at(m)
        gather_forward(hid_slot(j, q), hid_g(j, q))

    def mixed_out(k):
        gather_start(mixed_slot(k), mixed_g + k)

    def share():
        with jax.named_scope("shared"):
            block = tok[e].reshape(rows, width)
            shd[t] = silu_product(dot32(block, sg[...]), dot32(block, su[...]))

    def landed():
        for name in ("gw", "uw", "sg", "su", "dw"):
            loads[name].wait()

    acts = {
        "A": lambda m, q: arrive(m, q),
        "N": lambda m, q: arrive(m, q, crosses=False),
        "B": lambda m, q: crossed(m, q),
        "O": lambda m, q: own_crossed(q),
        "Z": lambda m, q: arrive_beside(m, q),
        "P": lambda m, q: inner_pair(q),
        "Q": lambda m, q: inner_far(q),
        "L": lambda m, q: own_late(),
        "H": lambda m, q: passed(m, q),
        "T": lambda m, q: [passed(m, each) for each in range(pieces)],
        "R": lambda m, q: relay(m, q),
        "M": lambda m, q: mixed_out(q),
        "X": lambda m, q: mix(),
        "W": lambda m, q: weigh(),
        "S": lambda m, q: share(),
        "D": lambda m, q: landed(),
        "E": lambda m, q: gate_block(e, 0, send=False),
        "K": lambda m, q: own_out(),
    }

    def table(names, r, k, unroll):
        found = jnp.int32(-1)
        for at, name in enumerate(names):
            if at % unroll == k and name != "--":
                found = jnp.where(r == at // unroll, int(name[0]) * pieces + int(name[1]), found)
        return found

    def due(part, r, k=0, unroll=1):
        for at, what in part.items():
            if at % unroll == k:

                @pl.when(r == at // unroll)
                def _():
                    for one in what:
                        acts[one[0]](int(one[1]), int(one[2]))

    def down_tiles(weight, hidden, place):
        part = hid.shape[-1]
        for c in range(chans // TILE):
            at = slice(c * TILE, (c + 1) * TILE)
            total = dot32(hidden(0), dw[0:part, at])
            for lane in range(1, n_tp):
                total += dot32(hidden(lane), dw[lane * part : (lane + 1) * part, at])
            place(at, (weight * total).astype(jnp.bfloat16))

    def down_piece(j, q):
        with jax.named_scope("hid_wait"):
            gather_finish(hid_slot(j, q), hid_g(j, q))

        def place(at, found):
            res[j, q, :, at] = found

        with jax.named_scope("down"):
            down_tiles(wcol[j, q][:, 0:1], lambda lane: hid[j, q, lane], place)
        for h in range(SUB):
            hop(j, q, h).start()

    def down_block(j, q):
        with jax.named_scope("hid_wait"):
            for q in range(pieces):
                gather_finish(hid_slot(j, q), hid_g(j, q))

        def place(at, found):
            res[j, :, :, at] = found.reshape(pieces, part_rows, TILE)

        with jax.named_scope("down"):
            down_tiles(
                wcol[j].reshape(rows, wcol.shape[-1])[:, 0:1],
                lambda lane: hid[j, :, lane].reshape(rows, hid.shape[-1]),
                place,
            )

    def gate_block(j, q, send=True):
        with jax.named_scope("gate_wait"):
            for q in range(pieces):
                gather_finish(tok_slot(j, q), j * pieces + q)

        with jax.named_scope("gate"):
            block = tok[j].reshape(rows, width)
            made = silu_product(dot32(block, gw[...]), dot32(block, uw[...]))
            made = made.reshape(n_tp, pieces, PIECE, made.shape[-1])
            for q in range(pieces):
                hid[j, q, t] = made[:, q].reshape(part_rows, made.shape[-1])
                if send:
                    gather_start(hid_slot(j, q), hid_g(j, q))

    def own_out():
        for q in range(pieces):
            gather_start(hid_slot(e, q), hid_g(e, q))
        gather_start(shd_slot, shared_g)

    def gate_piece(j, q):
        with jax.named_scope("gate_wait"):
            gather_finish(tok_slot(j, q), j * pieces + q)

        with jax.named_scope("gate"):
            block = tok[j, :, q].reshape(part_rows, width)
            hid[j, q, t] = silu_product(dot32(block, gw[...]), dot32(block, uw[...]))
            gather_start(hid_slot(j, q), hid_g(j, q))

    def run(plan, unroll, gate, down):
        def step(r, _):
            for k in range(unroll):
                with jax.named_scope("pre_down"):
                    due(plan["before_down"], r, k, unroll)
                if any(name != "--" for name in plan["downs"][k::unroll]):
                    down_at = table(plan["downs"], r, k, unroll)

                    @pl.when(down_at >= 0)
                    def _():
                        down(block_at(down_at // pieces), down_at % pieces)

                with jax.named_scope("pre_gate"):
                    due(plan["before_gate"], r, k, unroll)
                gate_at = table(plan["gates"], r, k, unroll)

                @pl.when(gate_at >= 0)
                def _():
                    gate(block_at(gate_at // pieces), gate_at % pieces)

                due(plan["after_gate"], r, k, unroll)

            return 0

        lax.fori_loop(0, -(-len(plan["gates"]) // unroll), step, 0)

    @pl.when(~inner)
    def _():
        run(END_PLAN, STEPS, gate_piece, down_piece)

    @pl.when(inner)
    def _():
        run(INNER_PLAN, 1, gate_block, down_block)

    @pl.when(~inner)
    def _():
        for q in range(pieces):
            passed(0, q)
        down_block(e, 0)

    @pl.when(inner)
    def _():
        for one in AFTER_STEPS:
            relay(int(one[0]), int(one[1]))

    with jax.named_scope("acc"):
        gather_forward(shd_slot, shared_g)
        loads["sd"].wait()
        gather_finish(shd_slot, shared_g)

        def shared_cols(c, _):
            at = pl.ds(pl.multiple_of(c * TILE, TILE), TILE)
            part = shd.shape[-1]
            total = dot32(shd[0], sd[0:part, at])
            for lane in range(1, n_tp):
                total += dot32(shd[lane], sd[lane * part : (lane + 1) * part, at])
            acc[:, :, :, at] = total.reshape(n_tp, pieces, PIECE, TILE)
            return 0

        lax.fori_loop(0, chans // TILE, shared_cols, 0)

    with jax.named_scope("mixed_wait"):
        loads["mw"].wait()
        for k in range(CHUNKS):
            gather_forward(mixed_slot(k), mixed_g + k)
        for k in range(CHUNKS):
            gather_finish(mixed_slot(k), mixed_g + k)

    def mixer_cols(c, _):
        with jax.named_scope("mixer"):
            at = pl.ds(pl.multiple_of(c * TILE, TILE), TILE)
            total = dot32(mixed[0], mw[0:chans, at])
            for lane in range(1, n_tp):
                total += dot32(mixed[lane], mw[lane * chans : (lane + 1) * chans, at])
            mix_out[:, at] = total.astype(jnp.bfloat16)


        @pl.when(inner)
        def _():
            due(BESIDE_MIXER, c)

        return 0

    lax.fori_loop(0, chans // TILE, mixer_cols, 0)

    def combine(q, _):
        with jax.named_scope("final_wait"):
            for here, slot in ((e > 0, e), (e < last, n_ep)):

                @pl.when(here)
                def _():
                    for h in range(SUB):
                        hop_arrives(slot, q, h)

        total = acc[:, q].reshape(part_rows, chans)
        for found in (res[e, q], pin[e, q], pin[n_ep, q]):
            total += found.astype(jnp.float32)
        whole = total.astype(jnp.bfloat16)
        for lane in range(n_tp):
            at = pl.ds(pl.multiple_of(lane * lane_rows + q * PIECE, PIECE), PIECE)
            exp_out[at, :] = whole[lane * PIECE : (lane + 1) * PIECE]
        return 0

    lax.fori_loop(0, pieces, combine, 0)

    @pl.when(e < last)
    def _():
        halo_copy().wait_send()

    def sent(ref, sem):
        remote(ref, ref, sem, h_sem.at[1], e, partner).wait_send()

    with jax.named_scope("drain"):

        @pl.when(~inner)
        def _():
            sent(tok.at[0, 0:n_x], z_send.at[0])

        @pl.when(inner)
        def _():
            sent(tok.at[0:2, 0], z_send.at[0])
            sent(tok.at[0 : n_ep - 2, 0], z_send.at[1])
            sent(tok.at[0, 0:n_x], z_send.at[2])

        sent(tok.at[0 : n_ep - 1, 0 : n_x - 1], x_send.at[0])
        sent(tok.at[:, 0:n_x], p_send.at[0])
        sent(hid.at[:, :, 0 : n_x - 1], x_send.at[1])
        sent(hid.at[:, :, 0:n_x], p_send.at[1])
        sent(shd.at[0 : n_x - 1], x_send.at[2])
        sent(shd.at[0:n_x], p_send.at[2])
        sent(mixed.at[0 : n_x - 1], x_send.at[3])
        sent(mixed.at[0:n_x], p_send.at[3])
        sent(res.at[0 : n_ep - 1], r_send.at[0])
        sent(wts.at[0 : n_ep - 1], w_send.at[0])


def joined(n_ep, n_tp, *args):
    (og, ig, va, taps, mw, ei, ng, ids, rw, gw, uw, dw, sg, su, sd) = args
    gw, uw, dw, ng = gw[0], uw[0], dw[0], ng[None]
    bf, f32 = jnp.bfloat16, jnp.float32
    rows, chans = og.shape
    lane_rows, width = ei.shape
    n_x = n_tp // CORES
    pieces = lane_rows // PIECE
    sems = 2 * n_ep * pieces + 1 + CHUNKS
    big = (og, ig, va, taps, mw, ei, ng, gw, uw, dw, sg, su, sd)
    out = pltpu.VMEM((rows, chans), bf)
    vmem = pl.BlockSpec(memory_space=pltpu.VMEM)
    dma = pltpu.SemaphoreType.DMA
    return pl.pallas_call(
        functools.partial(kernel, n_ep, n_tp),
        out_shape=(out, out),
        in_specs=[pl.BlockSpec(memory_space=pl.ANY)] * (2 + len(big)),
        out_specs=(vmem, vmem),
        scratch_shapes=[pltpu.VMEM(a.shape, a.dtype) for a in (*big, ids.T, rw.T)]
        + [
            pltpu.VMEM((n_ep, n_tp, pieces, PIECE, width), bf),
            pltpu.VMEM((n_ep, pieces, n_tp, n_tp * PIECE, gw.shape[-1]), bf),
            pltpu.VMEM((n_tp, rows, sg.shape[-1]), bf),
            pltpu.VMEM((n_tp, rows, chans), bf),
            pltpu.VMEM((rows, chans), bf),
            pltpu.VMEM((16, chans), bf),
            pltpu.VMEM((n_ep, pieces, n_tp * PIECE, chans), bf),
            pltpu.VMEM((n_ep + 1, pieces, n_tp * PIECE, chans), bf),
            pltpu.VMEM((n_tp, pieces, PIECE, chans), f32),
            pltpu.VMEM((n_ep, pieces, n_tp * PIECE, 128), f32),
            pltpu.VMEM((n_ep, -(-n_ep // 8) * 8, -(-rows // 128) * 128), f32),
            dma((len(big) + 1 + pieces,)),
            dma((3,)),
            dma((n_x, n_ep, pieces)),
            dma((4,)),
            dma((sems, max(1, n_x - 1))),
            dma((4,)),
            dma((sems, n_x)),
            dma((1,)),
            dma((n_ep + 1, pieces, SUB)),
            dma((1,)),
            dma((n_ep,)),
            dma((2,)),
        ],
        compiler_params=pltpu.CompilerParams(
            collective_id=0, has_side_effects=True, vmem_limit_bytes=60 * 1024 * 1024
        ),
    )(ids.T, rw.T, *big)


def local(*args):
    n_ep, n_tp = lax.axis_size("ep"), lax.axis_size("tp")
    chans, lane_rows = args[0].shape[1], args[5].shape[0]
    aligned = (
        n_tp % CORES == 0
        and n_ep == 2 * ROLES
        and lane_rows == STEPS * PIECE
        and lane_rows % PIECE == 0
        and lane_rows * n_tp == args[0].shape[0]
        and chans % TILE == 0
        and args[0].shape[0] % (16 * CHUNKS) == 0
        and args[9].shape[2] % 128 == 0
        and args[12].shape[1] % 128 == 0
    )
    return joined(n_ep, n_tp, *args) if aligned else plain(*args)


def solution(mesh):
    placed = (
        P(("grp", "ep"), "tp"),
        P(("grp", "ep"), "tp"),
        P(("grp", "ep"), "tp"),
        P(None, "tp"),
        P(None, "tp"),
        P(("grp", "ep", "tp"), None),
        P(),
        P(("grp", "ep"), None),
        P(("grp", "ep"), None),
        P("ep", None, "tp"),
        P("ep", None, "tp"),
        P("ep", None, "tp"),
        P(None, "tp"),
        P(None, "tp"),
        P(None, "tp"),
    )
    return jax.shard_map(
        local,
        mesh=mesh,
        in_specs=placed,
        out_specs=(P(("grp", "ep"), "tp"), P(("grp", "ep"), "tp")),
        check_vma=False,
    )
```

time: 73.8 us -> 65.6 us (0.89)
  Pallas kernels: 69.4 us -> 63.3 us
  local copies, waits for them, and re-layouts: 3.53 us -> 1.49 us
    pallas_call x1, Pallas kernels: 69.4 us -> 63.3 us  [joined(): pl.pallas_call(functools.partial(kernel, n_ep, n_tp), out_shape=(out, out...]
    unnamed x2, local copies, waits for them, and re-layouts: 3.53 us -> 1.49 us
where the time goes in v2:
time: 65.6 us; the launch traced here: 65.5 us
  Pallas kernels  63.3 us (96%)
  local copies, waits for them, and re-layouts  1.49 us (2%)
    pallas_call x1, Pallas kernels, joined(): pl.pallas_call(functools.partial(kernel, n_ep, n_tp), out_shape=(out, out...  63.3 us
    unnamed x2, local copies, waits for them, and re-layouts  1.49 us

profile of v2, /device:TPU:0, one launch (start us, length us, event | category | flops | bytes accessed | tf_op | source)
XLA Modules:
  0.0 65.5 jit_solution(52946141605755410)
XLA Ops:
  0.6 63.3 %shard_map.158 = (bf16[192,1024]{1,0:T(8,128)(2,1)S(1)}, bf16[192,1024]{1,0:T(8,128)(2,1)S(1)}) custom-call(s32[2,192]{1,0:T(2,128)} %bitcast.10, f32[2,192]{1,0:T(2,128)} %bitcast.11, bf16[192,1024]{1,0:T(8,128)(2,1)} %og_h.1, bf16[192,1024]{1,0:T(8,128)(2,1)} %ig_h.1, bf16[192,1024]{1,0:T(8,128)(2,1)} %va_h.1, f32[3,1024]{1,0:T(4,128)} %taps_h.1, ...), custom_call_target="tpu_custom_call" | custom-call | tf_op jit(solution)/shard_map/pallas_call | solution.py:824
  64.0 0.7 %copy.19 = bf16[192,1024]{1,0:T(8,128)(2,1)} copy(bf16[192,1024]{1,0:T(8,128)(2,1)S(1)} %get-tuple-element.2) | data formatting | bytes 786432
  64.7 0.7 %copy.20 = bf16[192,1024]{1,0:T(8,128)(2,1)} copy(bf16[192,1024]{1,0:T(8,128)(2,1)S(1)} %get-tuple-element.3) | data formatting | bytes 786432

commit v3 on v2

--- a/solution.py
+++ b/solution.py
@@ -13,53 +13,47 @@
 PIECE = 16
 CHUNKS = 4
 ROLES = 2
+MIX_TILES = 4
 STEPS = 3
-SUB = 1
+SUB = 2
 
 END_PLAN = dict(
-    gates=("20", "21", "22", "30", "31", "32", "10", "11", "12", "--", "--", "--"),
-    downs=("--", "--", "--", "20", "21", "22", "30", "31", "32", "10", "11", "12"),
+    gates=("20", "30", "21", "31", "--", "12", "32", "--", "22", "10", "11", "--", "--"),
+    downs=("--", "--", "--", "20", "30", "21", "--", "31", "32", "12", "22", "10", "11"),
     before_down={
+        0: ("c02", "c01", "u01", "u02", "A20", "A21", "O01", "D00", "O00", "O02", "N10", "B20", "A30", "E00"),
+        1: ("k01", "S00", "X00", "A31", "B30", "k02", "B21"),
+        3: ("H20", "A32", "B31", "W00"),
+        7: ("H31", "k00", "B22", "M03"),
+        10: ("H00", "M00", "N11", "M01", "H22", "Z11", "V03", "Y00"),
     },
     before_gate={
-        0: ("N10", "O00", "N11", "O01", "X00", "M00", "O02", "A20", "D00", "E00", "A21", "S00", "B20"),
-        1: ("A22", "W00", "B21"),
-        2: ("A30", "B22", "A31", "H20"),
-        3: ("A32", "B30", "H21"),
-        4: ("N12", "B31", "H22"),
-        5: ("Z10", "B32", "H30"),
-        6: ("H31",),
-        7: ("Z11", "H32"),
-        8: ("Z12", "H10"),
-        9: ("H11",),
-        10: ("H12",),
+        3: ("s00", "H30", "H21", "Z12"),
+        4: ("N12",),
+        5: ("A22", "B32"),
+        7: ("Z10", "M02", "H02", "U00", "H01", "H32", "H12"),
+        10: ("H10", "V02"),
+        11: ("V00", "C00", "H11", "V01"),
     },
-    after_gate={
-        5: ("M01",),
-        6: ("M02",),
-        7: ("M03",),
-        8: ("K00",),
-    },
+    after_gate={},
 )
 INNER_PLAN = dict(
-    gates=("20", "00", "30", "--", "--", "--", "--"),
-    downs=("--", "--", "--", "20", "00", "30", "10"),
+    gates=("00", "30", "20", "--", "--", "--"),
+    downs=("--", "--", "30", "00", "20", "10"),
     before_down={
-        3: ("T20",),
-        4: ("R20", "R21", "T00"),
-        5: ("T30",),
-        6: ("R22", "T10"),
+        0: ("c02", "u01", "c01", "a20", "a00", "a21", "b02", "a01", "a30", "a02", "a31", "b00", "u02", "a32", "B20", "l12", "X00", "B30", "Z01", "b01", "Z00", "D00", "Z02", "l02", "B31", "a22", "E00"),
+        1: ("B32",),
+        2: ("W00", "l10", "S00", "l01", "B21", "B22", "H31", "H00", "k00", "l11", "k01", "M03", "H32", "H30"),
     },
     before_gate={
-        0: ("P00", "P01", "P02", "X00", "W00", "D00", "E00", "Q00", "S00", "Q01", "Q02", "L00"),
-        2: ("B30", "B31", "B32"),
-        3: ("M00", "K00", "M01", "M02", "M03"),
+        2: ("R30", "H02", "H01"),
+        3: ("M00", "H10", "R31", "H20", "s00", "R00", "H22", "H11", "H21", "k02", "R32", "M02"),
+        4: ("R20", "M01", "V00", "H12", "R01", "R21", "V03", "U00"),
     },
-    after_gate={
-    },
+    after_gate={},
 )
-AFTER_STEPS = ("30", "31", "00", "32")
-BESIDE_MIXER = {0: ("R01",), 1: ("R02",)}
+END_AFTER = ("m00", "m01", "m02", "m03")
+INNER_AFTER = ("R02", "V01", "V02", "R22", "C00", "m00", "m01", "m02", "m03")
 
 norm_floor = 0.5
 
@@ -382,6 +376,9 @@
     def own_onward(side, d, q):
         z_copy(side, d, e, q, own=1).start()
 
+    def own_across(q):
+        gather_start(tok_slot(e, q), e * pieces + q)
+
     part_rows = n_tp * PIECE
     halves = part_rows // SUB
 
@@ -426,6 +423,16 @@
         spread_of = jnp.mean(centred * centred, axis=-1, keepdims=True)
         normed = centred * lax.rsqrt(spread_of + norm_floor) * ng[...]
         tok[e, t, q] = normed.astype(jnp.bfloat16)
+        if q == 0:
+            with jax.named_scope("barrier"):
+                pl.semaphore_wait(barrier, len(greeted))
+            own_onward(0, 0, q)
+
+            @pl.when(inner)
+            def _():
+                own_onward(1, 0, q)
+
+            own_across(q)
 
     for name, src, dst in (
         ("gw", gw_h, gw),
@@ -440,22 +447,6 @@
     ):
         load(name, src, dst)
 
-    with jax.named_scope("barrier"):
-        pl.semaphore_wait(barrier, len(greeted))
-
-    for q in range(pieces):
-        own_onward(0, 0, q)
-
-        if q < pieces - 1:
-
-            @pl.when(inner)
-            def _():
-                own_onward(1, 0, q)
-
-        for d in range(1, n_x):
-            cross(tok_slot(e, q), e * pieces + q, d, t).start()
-        across(tok_slot(e, q), e * pieces + q, 0, t).start()
-
     loads["ids"].wait()
     loads["rw"].wait()
     place = lax.broadcasted_iota(jnp.int32, (wts.shape[1], rows), 0)
@@ -536,24 +527,11 @@
         with jax.named_scope("weigh"):
             lax.fori_loop(0, n_ep, column, 0)
 
-    def own_late():
-        own_onward(1, 0, pieces - 1)
-        for d in range(1, n_x):
-            for q in range(pieces):
-                own_onward(1, d, q)
-
     def own_crossed(q):
         crossed(0, q, onward=0)
 
-    def inner_pair(q):
-        arrive(0, q, onward=0, crosses=False)
-        arrive(2, q, onward=1)
-        crossed(1, q)
-
-    def inner_far(q):
-        arrive(3, q, onward=1)
-        arrive_beside(0, q)
-        crossed(2, q)
+    def inner_arrive(m, q):
+        arrive(m, q, onward=0 if m == 0 else 1, crosses=m != 0)
 
     def passed(m, q):
         j = block_at(m)
@@ -571,25 +549,62 @@
         for name in ("gw", "uw", "sg", "su", "dw"):
             loads[name].wait()
 
+    def shared_down():
+        with jax.named_scope("acc"):
+            loads["sd"].wait()
+            gather_finish(shd_slot, shared_g)
+
+            def shared_cols(c, _):
+                at = pl.ds(pl.multiple_of(c * TILE, TILE), TILE)
+                part = shd.shape[-1]
+                total = dot32(shd[0], sd[0:part, at])
+                for lane in range(1, n_tp):
+                    total += dot32(shd[lane], sd[lane * part : (lane + 1) * part, at])
+                acc[:, :, :, at] = total.reshape(n_tp, pieces, PIECE, TILE)
+                return 0
+
+            lax.fori_loop(0, chans // TILE, shared_cols, 0)
+
+    def mixer_tile(c):
+        if c == 0:
+            with jax.named_scope("mixed_wait"):
+                loads["mw"].wait()
+                for k in range(CHUNKS):
+                    gather_finish(mixed_slot(k), mixed_g + k)
+
+        with jax.named_scope("mixer"):
+            at = pl.ds(c * TILE, TILE)
+            total = dot32(mixed[0], mw[0:chans, at])
+            for lane in range(1, n_tp):
+                total += dot32(mixed[lane], mw[lane * chans : (lane + 1) * chans, at])
+            mix_out[:, at] = total.astype(jnp.bfloat16)
+
     acts = {
         "A": lambda m, q: arrive(m, q),
         "N": lambda m, q: arrive(m, q, crosses=False),
+        "a": lambda m, q: inner_arrive(m, q),
         "B": lambda m, q: crossed(m, q),
         "O": lambda m, q: own_crossed(q),
+        "b": lambda m, q: crossed(1, q),
         "Z": lambda m, q: arrive_beside(m, q),
-        "P": lambda m, q: inner_pair(q),
-        "Q": lambda m, q: inner_far(q),
-        "L": lambda m, q: own_late(),
+        "l": lambda m, q: own_onward(1, m, q),
         "H": lambda m, q: passed(m, q),
-        "T": lambda m, q: [passed(m, each) for each in range(pieces)],
         "R": lambda m, q: relay(m, q),
         "M": lambda m, q: mixed_out(q),
+        "V": lambda m, q: gather_forward(mixed_slot(q), mixed_g + q),
         "X": lambda m, q: mix(),
         "W": lambda m, q: weigh(),
-        "S": lambda m, q: share(),
         "D": lambda m, q: landed(),
         "E": lambda m, q: gate_block(e, 0, send=False),
-        "K": lambda m, q: own_out(),
+        "k": lambda m, q: gather_start(hid_slot(e, q), hid_g(e, q)),
+        "S": lambda m, q: share(),
+        "s": lambda m, q: gather_start(shd_slot, shared_g),
+        "U": lambda m, q: gather_forward(shd_slot, shared_g),
+        "u": lambda m, q: own_onward(0, 0, q),
+        "c": lambda m, q: own_across(q),
+        "Y": lambda m, q: down_block(e, 0),
+        "C": lambda m, q: shared_down(),
+        "m": lambda m, q: mixer_tile(q),
     }
 
     def table(names, r, k, unroll):
@@ -658,11 +673,6 @@
                 if send:
                     gather_start(hid_slot(j, q), hid_g(j, q))
 
-    def own_out():
-        for q in range(pieces):
-            gather_start(hid_slot(e, q), hid_g(e, q))
-        gather_start(shd_slot, shared_g)
-
     def gate_piece(j, q):
         with jax.named_scope("gate_wait"):
             gather_finish(tok_slot(j, q), j * pieces + q)
@@ -706,56 +716,12 @@
     def _():
         run(INNER_PLAN, 1, gate_block, down_block)
 
-    @pl.when(~inner)
-    def _():
-        for q in range(pieces):
-            passed(0, q)
-        down_block(e, 0)
-
-    @pl.when(inner)
-    def _():
-        for one in AFTER_STEPS:
-            relay(int(one[0]), int(one[1]))
-
-    with jax.named_scope("acc"):
-        gather_forward(shd_slot, shared_g)
-        loads["sd"].wait()
-        gather_finish(shd_slot, shared_g)
-
-        def shared_cols(c, _):
-            at = pl.ds(pl.multiple_of(c * TILE, TILE), TILE)
-            part = shd.shape[-1]
-            total = dot32(shd[0], sd[0:part, at])
-            for lane in range(1, n_tp):
-                total += dot32(shd[lane], sd[lane * part : (lane + 1) * part, at])
-            acc[:, :, :, at] = total.reshape(n_tp, pieces, PIECE, TILE)
-            return 0
-
-        lax.fori_loop(0, chans // TILE, shared_cols, 0)
-
-    with jax.named_scope("mixed_wait"):
-        loads["mw"].wait()
-        for k in range(CHUNKS):
-            gather_forward(mixed_slot(k), mixed_g + k)
-        for k in range(CHUNKS):
-            gather_finish(mixed_slot(k), mixed_g + k)
-
-    def mixer_cols(c, _):
-        with jax.named_scope("mixer"):
-            at = pl.ds(pl.multiple_of(c * TILE, TILE), TILE)
-            total = dot32(mixed[0], mw[0:chans, at])
-            for lane in range(1, n_tp):
-                total += dot32(mixed[lane], mw[lane * chans : (lane + 1) * chans, at])
-            mix_out[:, at] = total.astype(jnp.bfloat16)
-
-
-        @pl.when(inner)
+    for here, after in ((~inner, END_AFTER), (inner, INNER_AFTER)):
+
+        @pl.when(here)
         def _():
-            due(BESIDE_MIXER, c)
-
-        return 0
-
-    lax.fori_loop(0, chans // TILE, mixer_cols, 0)
+            for one in after:
+                acts[one[0]](int(one[1]), int(one[2]))
 
     def combine(q, _):
         with jax.named_scope("final_wait"):
@@ -865,6 +831,7 @@
         n_tp % CORES == 0
         and n_ep == 2 * ROLES
         and lane_rows == STEPS * PIECE
+        and chans == MIX_TILES * TILE
         and lane_rows % PIECE == 0
         and lane_rows * n_tp == args[0].shape[0]
         and chans % TILE == 0

time: 65.6 us -> 62.2 us (0.948); the launches traced: 65.5 us -> 61 us
  Pallas kernels: 63.3 us -> 58.8 us
    pallas_call x1, Pallas kernels: 63.3 us -> 58.8 us  [joined(): pl.pallas_call(functools.partial(kernel, n_ep, n_tp), out_shape=(out, out...]
where the time goes in v3:
time: 62.2 us; the launch traced here: 61 us
  Pallas kernels  58.8 us (95%)
  local copies, waits for them, and re-layouts  1.49 us (2%)
  between operations  0.65 us (1%)
    pallas_call x1, Pallas kernels, joined(): pl.pallas_call(functools.partial(kernel, n_ep, n_tp), out_shape=(out, out...  58.8 us
    unnamed x2, local copies, waits for them, and re-layouts  1.49 us

profile of v3, /device:TPU:0, one launch (start us, length us, event | category | flops | bytes accessed | tf_op | source)
XLA Modules:
  0.0 61.0 jit_solution(3662156531473032512)
XLA Ops:
  0.6 58.8 %shard_map.158 = (bf16[192,1024]{1,0:T(8,128)(2,1)S(1)}, bf16[192,1024]{1,0:T(8,128)(2,1)S(1)}) custom-call(s32[2,192]{1,0:T(2,128)} %bitcast.10, f32[2,192]{1,0:T(2,128)} %bitcast.11, bf16[192,1024]{1,0:T(8,128)(2,1)} %og_h.1, bf16[192,1024]{1,0:T(8,128)(2,1)} %ig_h.1, bf16[192,1024]{1,0:T(8,128)(2,1)} %va_h.1, f32[3,1024]{1,0:T(4,128)} %taps_h.1, ...), custom_call_target="tpu_custom_call" | custom-call | tf_op jit(solution)/shard_map/pallas_call | solution.py:790
  59.5 0.7 %copy.19 = bf16[192,1024]{1,0:T(8,128)(2,1)} copy(bf16[192,1024]{1,0:T(8,128)(2,1)S(1)} %get-tuple-element.2) | data formatting | bytes 786432
  60.2 0.7 %copy.20 = bf16[192,1024]{1,0:T(8,128)(2,1)} copy(bf16[192,1024]{1,0:T(8,128)(2,1)S(1)} %get-tuple-element.3) | data formatting | bytes 786432
